TPU v7x, 512 devices: a whole 4x8x8 slice. The times are simulated.
512 devices in a mesh: fs: 64 (over z, y), rep: 4 (over x), tp: 2 (over core).
Axes of the slice: x: 4, y: 8, z: 8, core: 2. Of those that a mesh axis runs over, the one named last changes fastest.
Arguments:
- attention_input: bfloat16 [196608, 2048], P(('fs', 'rep')), may hold values from -6 to 6
- query_cotangent: bfloat16 [196608, 1024], P(('fs', 'rep'), 'tp'), may hold values from -15 to 15
- gate_cotangent: float32 [16, 196608], P('tp', ('fs', 'rep')), may hold values from -6 to 6
- gate_totals: float32 [16, 196608], P('tp', ('fs', 'rep')), may hold values from -2304 to 0, as said below
- projector: bfloat16 [2048, 256], P('fs'), may hold values from -1 to 1
- query_master: float32 [2048, 1024], P('fs', 'tp'), may hold values from -0.125 to 0.125
- lowrank_mean: float32 [256, 1024], P('rep', 'tp'), may hold values from -32 to 32
- lowrank_square: float32 [256, 1024], P('rep', 'tp'), may hold values from 0.05 to 2
- gating_mean: float32 [16, 2048], P('tp'), may hold values from -1.8 to 1.8
- gating_square: float32 [16, 2048], P('tp'), may hold values from 0.01 to 1
Outputs:
- query_update: float32 [2048, 1024], P('fs', 'tp')
- query_renewed: float32 [2048, 1024], P('fs', 'tp')
- query_copy: bfloat16 [2048, 1024], P('fs', 'tp')
- mean_after: float32 [256, 1024], P('rep', 'tp')
- square_after: float32 [256, 1024], P('rep', 'tp')
- gating_update: float32 [16, 2048], P('tp')
- gating_average: float32 [16, 2048], P('tp')
- gating_energy: float32 [16, 2048], P('tp')
Inputs may be any that keep to these rules, and one draw needn't show every extreme that they name: `gate_totals`: within each sequence of 768 positions, a running sum of negative log gates, so successive differences are negative.
All inputs are finite; a program needn't handle non-finite values.
Results may differ from a plain program's by a relative error of at most 0.0044.
The roundings to bfloat16 on the way count: a program that leaves them out, or rounds other values in their place, can miss the bound.
Values may be sent and summed in bfloat16 or wider, within the bound.
No kernel may reach another device: no remote copies, remote signals or barrier semaphores. Data moves between devices by JAX's collectives and lax.ppermute only.
A program may use at most 64 MiB of HBM per device.

v0:
```python
import jax
import jax.numpy as jnp
from jax import lax
from jax.sharding import Mesh
from jax.sharding import PartitionSpec as P

FS = ("fs_0", "fs_1")
FS_REP = ("fs_0", "fs_1", "rep")


BETA_ONE = 0.9
BETA_TWO = 0.95
STEP_RATE = 0.01
EPSILON = 1e-08
NORM_FLOOR = 1e-06


def cut_along(value, dim, length):
    before, after = (value.shape[:dim], value.shape[dim + 1 :])
    return jnp.moveaxis(value.reshape(*before, length, -1, *after), dim, 0)


def sent_and_summed(value, axis, dim):
    length = lax.axis_size(axis)
    pieces = lax.all_to_all(cut_along(value, dim, length), axis, 0, 0, tiled=True)
    return jnp.sum(pieces, axis=0)


def sum_by_axis(value, axes, dim):
    far, near = axes
    own = sent_and_summed(cut_along(value, dim, lax.axis_size(far)), near, dim + 1)
    return jnp.sum(lax.all_to_all(own, far, 0, 0, tiled=True), axis=0)


def rows_for(lines, length):
    spare = -len(lines) % length
    return jnp.pad(lines, [(0, spare)] + [(0, 0)] * (lines.ndim - 1))


def from_everyone(value, axis):
    length = lax.axis_size(axis)
    return lax.all_to_all(
        jnp.broadcast_to(value[None], (length, *value.shape)), axis, 0, 0, tiled=True
    )


def in_order(pieces, dim):
    lengths = list(pieces.shape[1:])
    lengths[dim] *= pieces.shape[0]
    return jnp.moveaxis(pieces, 0, dim).reshape(lengths)


def gather_axes(value, axes, dim):
    far, near = axes
    initial = from_everyone(value, far)
    pieces = jnp.swapaxes(from_everyone(initial, near), 0, 1)
    return in_order(pieces.reshape(-1, *value.shape), dim)


def nested_sum(value, axes):
    lines = value.reshape(-1)
    own = sum_by_axis(rows_for(lines, lax.axis_size(axes[0]) * lax.axis_size(axes[1])), axes, 0)
    whole = gather_axes(own, axes, 0)
    return whole[: len(lines)].reshape(value.shape)


def sum_by_axis_2(running, axes):
    for axis in axes:
        running = lax.psum_scatter(running, axis, scatter_dimension=0, tiled=True)
    return running


def over_copies(value, axis):
    return from_everyone(value, axis).sum(axis=0)


def gathered_copies(value, axis, dim):
    return in_order(from_everyone(value, axis), dim)


def sum_by_parts(value, axes):
    lines = value.reshape(-1, value.shape[-1])
    padded = rows_for(lines, lax.axis_size(axes))
    whole = gathered_copies(sent_and_summed(padded, axes, 0), axes, 0)
    return lax.slice_in_dim(whole, 0, len(lines)).reshape(value.shape)


def packed_total(arrays, axis):
    ends = [0]
    for a in arrays:
        ends.append(ends[-1] + a.size)
    running = over_copies(jnp.concatenate([a.ravel() for a in arrays]), axis)
    return tuple((running[b:e].reshape(a.shape) for a, b, e in zip(arrays, ends, ends[1:])))


def per_device(
    attention_input,
    query_cotangent,
    gate_cotangent,
    gate_totals,
    projector,
    query_master,
    lowrank_mean,
    lowrank_square,
    gating_mean,
    gating_square,
):
    tokens_all = attention_input.shape[0] * lax.axis_size(FS) * lax.axis_size("rep")
    norming = 1.0 / tokens_all**0.5
    contract = (((0,), (0,)), ((), ()))
    earlier = jnp.concatenate(
        [jnp.zeros((gate_totals.shape[0], 1), jnp.float32), gate_totals[:, :-1]], axis=1
    )
    gate_logarithm = gate_totals - earlier
    trailing = lax.cumsum(gate_cotangent, axis=1, reverse=True)
    gate_signal = (trailing * -jnp.expm1(gate_logarithm)).astype(jnp.bfloat16)
    gate_partial = jnp.dot(gate_signal, attention_input, preferred_element_type=jnp.float32)
    forget_gradient = nested_sum(gate_partial, (("fs_0", "fs_1"), "rep")) * norming
    partial_rows = sum_by_axis_2(
        lax.dot_general(
            attention_input, query_cotangent, contract, preferred_element_type=jnp.float32
        ),
        FS,
    )
    gradient = over_copies(partial_rows, "rep") * norming
    rank_rows = lowrank_mean.shape[0]
    own_factor = lax.dynamic_slice_in_dim(
        projector, lax.axis_index("rep") * rank_rows, rank_rows, 1
    ).astype(jnp.float32)
    rank_partial = lax.dot_general(
        own_factor,
        gradient,
        contract,
        precision=lax.Precision.HIGHEST,
        preferred_element_type=jnp.float32,
    )
    projected = sum_by_parts(rank_partial, FS)
    mean_after = BETA_ONE * lowrank_mean + (1.0 - BETA_ONE) * projected
    square_after = BETA_TWO * lowrank_square + (1.0 - BETA_TWO) * projected * projected
    direction = mean_after / (jnp.sqrt(square_after) + EPSILON)
    direction_squares, projected_squares = packed_total(
        (jnp.sum(direction * direction), jnp.sum(projected * projected)), ("rep", "tp")
    )
    balance = jnp.sqrt(direction_squares / (projected_squares + NORM_FLOOR))
    blended = (direction - balance * projected).astype(jnp.bfloat16)
    lifted = jnp.dot(
        projector, gathered_copies(blended, "rep", 0), preferred_element_type=jnp.float32
    )
    query_update = lifted + balance * gradient
    query_renewed = query_master - STEP_RATE * query_update
    query_copy = query_renewed.astype(jnp.bfloat16)
    gating_average = BETA_ONE * gating_mean + (1.0 - BETA_ONE) * forget_gradient
    gating_energy = BETA_TWO * gating_square + (1.0 - BETA_TWO) * forget_gradient * forget_gradient
    gating_update = gating_average / (jnp.sqrt(gating_energy) + EPSILON)
    return (
        query_update,
        query_renewed,
        query_copy,
        mean_after,
        square_after,
        gating_update,
        gating_average,
        gating_energy,
    )


def solution(mesh):
    split = Mesh(
        mesh.devices.reshape(8, 8, mesh.shape["rep"], mesh.shape["tp"]),
        ("fs_0", "fs_1", "rep", "tp"),
    )
    in_specs = (
        P(FS_REP, None),
        P(FS_REP, "tp"),
        P("tp", FS_REP),
        P("tp", FS_REP),
        P(FS, None),
        P(FS, "tp"),
        P("rep", "tp"),
        P("rep", "tp"),
        P("tp", None),
        P("tp", None),
    )
    out_specs = (
        P(FS, "tp"),
        P(FS, "tp"),
        P(FS, "tp"),
        P("rep", "tp"),
        P("rep", "tp"),
        P("tp", None),
        P("tp", None),
        P("tp", None),
    )
    return jax.shard_map(
        per_device, mesh=split, in_specs=in_specs, out_specs=out_specs, check_vma=False
    )
```

profile of v0, /device:TPU:1, one launch (start us, length us, event | category | flops | bytes accessed | tf_op | source)
XLA Modules:
  0.0 236.5 jit_solution(868699480572917151)
XLA Ops:
  7.2 1.8 copy-done
  9.1 4.9 %fusion.20 = f32[2048,512]{1,0:T(8,128)} fusion(bf16[768,2048]{1,0:T(8,128)(2,1)S(1)} %copy-done, bf16[768,512]{1,0:T(8,128)(2,1)} %param.11), kind=kOutput, calls=%fused_computation.34 | convolution fusion | flops 1610612736 | bytes 8126464 | tf_op jit(solution)/shard_map/dot_general | solution.py:120
  14.0 64.3 %reduce-scatter.3.cloned.1.call-done = f32[256,512]{1,0:T(8,128)} async-done(((f32[2048,512]{1,0:T(8,128)}), f32[256,512]{1,0:T(8,128)}) %reduce-scatter.3.cloned.1.call-update) | async-done | bytes 524304 | tf_op jit(solution)/shard_map/reduce_scatter | solution.py:69
  78.4 7.4 %reduce-window.6 = f32[8,6,128]{2,0,1:T(8,128)S(1)} reduce-window(f32[8,6,128]{2,0,1:T(8,128)S(1)} %bitcast.54, f32[]{:T(128)} %constant.6.clone.1), window={size=1x1x128 pad=0_0x0_0x0_127}, to_apply=%region_7.8 | reduce-window | flops 780288 | bytes 49156 | tf_op jit(solution)/shard_map/reduce-window
  85.8 0.1 copy.38
  86.0 0.2 reduce-window.9
  86.3 0.6 fusion.9
  87.1 8.2 %all_to_all.51 = f32[4,1,4096]{2,1,0:T(1,128)S(1)} all-to-all(f32[4,1,4096]{2,1,0:T(1,128)S(1)} %reshape.86), channel_id=1, replica_groups=mesh['fs_0'=8,'fs_1'=8,'rep'=4,'tp'=2] {'rep'}, dimensions={0} | all-to-all | bytes 131072 | tf_op jit(solution)/shard_map/all_to_all | solution.py:25
  95.4 0.5 broadcast.37
  95.9 0.8 reduce.3
  96.7 0.1 reshape.87
  96.8 20.4 %all_to_all.52 = f32[64,1,64]{2,1,0:T(1,128)S(1)} all-to-all(f32[64,1,64]{2,1,0:T(1,128)S(1)} %bitcast.52), channel_id=1, replica_groups=mesh['fs_0'=8,'fs_1'=8,'rep'=4,'tp'=2] {'fs_0','fs_1'}, dimensions={0} | all-to-all | bytes 32768 | tf_op jit(solution)/shard_map/all_to_all | solution.py:32
  117.3 1.6 broadcast_in_dim.14
  118.8 3.4 %all-to-all-start = ((f32[4,32,512]{2,1,0:T(8,128)}), f32[4,32,512]{2,1,0:T(8,128)S(1)}, u32[]{:S(2)}, u32[]{:S(2)}) async-start(f32[4,32,512]{2,1,0:T(8,128)} %broadcast_in_dim.14), calls=%async_computation.2 | async-start | bytes 524288 | tf_op jit(solution)/shard_map/all_to_all | solution.py:42
  122.3 5.4 %all-to-all-done = f32[4,32,512]{2,1,0:T(8,128)S(1)} async-done(((f32[4,32,512]{2,1,0:T(8,128)}), f32[4,32,512]{2,1,0:T(8,128)S(1)}, u32[]{:S(2)}, u32[]{:S(2)}) %all-to-all-start) | async-done | bytes 262176 | tf_op jit(solution)/shard_map/all_to_all | solution.py:42
  127.7 0.6 broadcast_in_dim.18
  128.4 9.0 %all-to-all-start.7 = ((f32[64,1,64]{2,1,0:T(1,128)}), f32[64,1,64]{2,1,0:T(1,128)S(1)}, u32[]{:S(2)}, u32[]{:S(2)}) async-start(f32[64,1,64]{2,1,0:T(1,128)} %broadcast_in_dim.18), calls=%async_computation.9 | async-start | bytes 65536 | tf_op jit(solution)/shard_map/all_to_all | solution.py:42
  137.4 0.3 convolution_bitcast_fusion
  137.8 0.8 copy.36
  138.6 9.6 %all-to-all-done.7 = f32[64,1,64]{2,1,0:T(1,128)S(1)} async-done(((f32[64,1,64]{2,1,0:T(1,128)}), f32[64,1,64]{2,1,0:T(1,128)S(1)}, u32[]{:S(2)}, u32[]{:S(2)}) %all-to-all-start.7) | async-done | bytes 16416 | tf_op jit(solution)/shard_map/all_to_all | solution.py:42
  148.2 4.6 %all-to-all-start.1 = ((f32[64,1,512]{2,1,0:T(1,128)}), f32[64,1,512]{2,1,0:T(1,128)S(1)}, u32[]{:S(2)}, u32[]{:S(2)}) async-start(f32[64,1,512]{2,1,0:T(1,128)} %copy.36), calls=%async_computation.3 | async-start | bytes 262144 | tf_op jit(solution)/shard_map/all_to_all | solution.py:25
  152.8 0.8 reshape.88
  153.6 10.8 %all-to-all-done.1 = f32[64,1,512]{2,1,0:T(1,128)S(1)} async-done(((f32[64,1,512]{2,1,0:T(1,128)}), f32[64,1,512]{2,1,0:T(1,128)S(1)}, u32[]{:S(2)}, u32[]{:S(2)}) %all-to-all-start.1) | async-done | bytes 131104 | tf_op jit(solution)/shard_map/all_to_all | solution.py:25
  164.4 3.3 %all-to-all-start.8 = ((f32[4,1,4096]{2,1,0:T(1,128)}), f32[4,1,4096]{2,1,0:T(1,128)S(1)}, u32[]{:S(2)}, u32[]{:S(2)}) async-start(f32[4,1,4096]{2,1,0:T(1,128)} %reshape.88), calls=%async_computation.10 | async-start | bytes 131072 | tf_op jit(solution)/shard_map/all_to_all | solution.py:42
  167.8 4.6 %all-to-all-done.8 = f32[4,1,4096]{2,1,0:T(1,128)S(1)} async-done(((f32[4,1,4096]{2,1,0:T(1,128)}), f32[4,1,4096]{2,1,0:T(1,128)S(1)}, u32[]{:S(2)}, u32[]{:S(2)}) %all-to-all-start.8) | async-done | bytes 65568 | tf_op jit(solution)/shard_map/all_to_all | solution.py:42
  172.4 0.7 broadcast_in_dim.15
  173.1 4.6 %all-to-all-start.2 = ((f32[64,1,512]{2,1,0:T(1,128)}), f32[64,1,512]{2,1,0:T(1,128)S(1)}, u32[]{:S(2)}, u32[]{:S(2)}) async-start(f32[64,1,512]{2,1,0:T(1,128)} %broadcast_in_dim.15), calls=%async_computation.4 | async-start | bytes 262144 | tf_op jit(solution)/shard_map/all_to_all | solution.py:42
  177.7 0.8 reduce.4
  178.6 0.8 reshape.89
  179.3 0.9 multiply_bitcast_fusion.1
  180.3 0.7 copy.42
  181.0 1.1 mul.150
  182.1 0.7 copy.41
  182.8 6.5 %all-to-all-done.2 = f32[64,1,512]{2,1,0:T(1,128)S(1)} async-done(((f32[64,1,512]{2,1,0:T(1,128)}), f32[64,1,512]{2,1,0:T(1,128)S(1)}, u32[]{:S(2)}, u32[]{:S(2)}) %all-to-all-start.2) | async-done | bytes 131104 | tf_op jit(solution)/shard_map/all_to_all | solution.py:42
  189.3 2.3 multiply_reduce_fusion
  191.6 1.4 pad_maximum_fusion
  193.0 0.6 broadcast_in_dim.16
  193.6 14.9 %all-to-all-start.3 = ((f32[8,1,2]{2,1,0:T(1,128)}), f32[8,1,2]{2,1,0:T(1,128)}, u32[]{:S(2)}, u32[]{:S(2)}) async-start(f32[8,1,2]{2,1,0:T(1,128)} %broadcast_in_dim.16), calls=%async_computation.5 | async-start | bytes 8192 | tf_op jit(solution)/shard_map/all_to_all | solution.py:42
  208.5 1.7 mul.141
  210.2 3.0 %all-to-all-done.3 = f32[8,1,2]{2,1,0:T(1,128)} async-done(((f32[8,1,2]{2,1,0:T(1,128)}), f32[8,1,2]{2,1,0:T(1,128)}, u32[]{:S(2)}, u32[]{:S(2)}) %all-to-all-start.3) | async-done | bytes 96 | tf_op jit(solution)/shard_map/all_to_all | solution.py:42
  213.1 1.2 reduce_sum.67
  214.3 1.3 fusion.19
  217.0 1.0 fusion.4
  218.0 0.7 broadcast_in_dim.17
  218.7 3.4 %all-to-all-start.4 = ((bf16[4,64,512]{2,1,0:T(8,128)(2,1)}), bf16[4,64,512]{2,1,0:T(8,128)(2,1)S(1)}, u32[]{:S(2)}, u32[]{:S(2)}) async-start(bf16[4,64,512]{2,1,0:T(8,128)(2,1)} %broadcast_in_dim.17), calls=%async_computation.6 | async-start | bytes 524288 | tf_op jit(solution)/shard_map/all_to_all | solution.py:42
  222.1 1.6 add_divide_fusion.1
  223.7 4.3 %all-to-all-done.4 = bf16[4,64,512]{2,1,0:T(8,128)(2,1)S(1)} async-done(((bf16[4,64,512]{2,1,0:T(8,128)(2,1)}), bf16[4,64,512]{2,1,0:T(8,128)(2,1)S(1)}, u32[]{:S(2)}, u32[]{:S(2)}) %all-to-all-start.4) | async-done | bytes 262176 | tf_op jit(solution)/shard_map/all_to_all | solution.py:42
  228.0 1.7 fusion.16
  (24 shorter events, 0.8 us)
Async XLA Ops:
  7.2 1.9 copy-start
  7.2 71.1 %reduce-scatter.3.cloned.1.call-start = ((), (), s32[]{:S(2)}) async-start(), calls=%async_computation.11 | async-start | bytes 4718592 | tf_op jit(solution)/shard_map/reduce_scatter | solution.py:69
  13.9 64.4 %copy-start.4 = (f32[8,768]{1,0:T(8,128)S(1)}, f32[8,768]{1,0:T(8,128)}, u32[]{:S(2)}) copy-start(f32[8,768]{1,0:T(8,128)} %param.12) | copy-start | bytes 73732
  14.0 72.3 %copy-start.2 = (f32[8,768]{1,0:T(8,128)S(1)}, f32[8,768]{1,0:T(8,128)}, u32[]{:S(2)}) copy-start(f32[8,768]{1,0:T(8,128)} %param.13) | copy-start | bytes 73732
  14.0 103.3 %reduce-scatter.5.cloned.1.call-start = ((), (), s32[]{:S(2)}) async-start(), calls=%async_computation.12 | async-start | bytes 589824 | tf_op jit(solution)/shard_map/reduce_scatter | solution.py:69
  78.3 59.1 %copy-start.3 = (bf16[32,256]{1,0:T(8,128)(2,1)S(1)}, bf16[32,256]{1,0:T(8,128)(2,1)}, u32[]{:S(2)}) copy-start(bf16[32,256]{1,0:T(8,128)(2,1)} %param.14) | copy-start | bytes 49156
  118.8 8.9 %all-to-all-start = ((f32[4,32,512]{2,1,0:T(8,128)}), f32[4,32,512]{2,1,0:T(8,128)S(1)}, u32[]{:S(2)}, u32[]{:S(2)}) async-start(f32[4,32,512]{2,1,0:T(8,128)} %broadcast_in_dim.14), calls=%async_computation.2 | async-start | bytes 524288 | tf_op jit(solution)/shard_map/all_to_all | solution.py:42
  128.4 19.8 %all-to-all-start.7 = ((f32[64,1,64]{2,1,0:T(1,128)}), f32[64,1,64]{2,1,0:T(1,128)S(1)}, u32[]{:S(2)}, u32[]{:S(2)}) async-start(f32[64,1,64]{2,1,0:T(1,128)} %broadcast_in_dim.18), calls=%async_computation.9 | async-start | bytes 65536 | tf_op jit(solution)/shard_map/all_to_all | solution.py:42
  148.2 16.2 %all-to-all-start.1 = ((f32[64,1,512]{2,1,0:T(1,128)}), f32[64,1,512]{2,1,0:T(1,128)S(1)}, u32[]{:S(2)}, u32[]{:S(2)}) async-start(f32[64,1,512]{2,1,0:T(1,128)} %copy.36), calls=%async_computation.3 | async-start | bytes 262144 | tf_op jit(solution)/shard_map/all_to_all | solution.py:25
  164.4 8.0 %all-to-all-start.8 = ((f32[4,1,4096]{2,1,0:T(1,128)}), f32[4,1,4096]{2,1,0:T(1,128)S(1)}, u32[]{:S(2)}, u32[]{:S(2)}) async-start(f32[4,1,4096]{2,1,0:T(1,128)} %reshape.88), calls=%async_computation.10 | async-start | bytes 131072 | tf_op jit(solution)/shard_map/all_to_all | solution.py:42
  173.1 16.2 %all-to-all-start.2 = ((f32[64,1,512]{2,1,0:T(1,128)}), f32[64,1,512]{2,1,0:T(1,128)S(1)}, u32[]{:S(2)}, u32[]{:S(2)}) async-start(f32[64,1,512]{2,1,0:T(1,128)} %broadcast_in_dim.15), calls=%async_computation.4 | async-start | bytes 262144 | tf_op jit(solution)/shard_map/all_to_all | solution.py:42
  191.6 27.1 %copy-start.1 = (f32[64,512]{1,0:T(8,128)}, f32[64,512]{1,0:T(8,128)S(1)}, u32[]{:S(2)}) copy-start(f32[64,512]{1,0:T(8,128)S(1)} %get-tuple-element.14) | copy-start | bytes 393220
  193.6 19.6 %all-to-all-start.3 = ((f32[8,1,2]{2,1,0:T(1,128)}), f32[8,1,2]{2,1,0:T(1,128)}, u32[]{:S(2)}, u32[]{:S(2)}) async-start(f32[8,1,2]{2,1,0:T(1,128)} %broadcast_in_dim.16), calls=%async_computation.5 | async-start | bytes 8192 | tf_op jit(solution)/shard_map/all_to_all | solution.py:42
  218.7 9.3 %all-to-all-start.4 = ((bf16[4,64,512]{2,1,0:T(8,128)(2,1)}), bf16[4,64,512]{2,1,0:T(8,128)(2,1)S(1)}, u32[]{:S(2)}, u32[]{:S(2)}) async-start(bf16[4,64,512]{2,1,0:T(8,128)(2,1)} %broadcast_in_dim.17), calls=%async_computation.6 | async-start | bytes 524288 | tf_op jit(solution)/shard_map/all_to_all | solution.py:42
Sparse Core Ops, SparseCore 0:
  14.1 64.1 reduce-scatter.2
  81.1 33.6 reduce-scatter.4
where the time goes:
time: 238 us; the launch traced here: 236 us
  waiting for transfers between devices  108 us (45%)
  starting transfers between devices  43.4 us (18%)
  blocking collectives  28.7 us (12%)
  other arithmetic  17.8 us (7%)
  between operations  15.5 us (7%)
  local copies, waits for them, and re-layouts  15.1 us (6%)
  matrix products  7.43 us (3%)
    reduce_scatter x2, waiting for transfers between devices, sum_by_axis_2(): running = lax.psum_scatter(running, axis, scatter_dimension=0, tiled=True)  64.3 us
    all_to_all x6, starting transfers between devices, from_everyone(): lax.all_to_all(jnp.broadcast_to(value[None], (length, *value.shape)), axi...  38.7 us
    all_to_all x6, waiting for transfers between devices, from_everyone(): lax.all_to_all(jnp.broadcast_to(value[None], (length, *value.shape)), axi...  33.4 us
    all_to_all x1, blocking collectives, sum_by_axis(): return jnp.sum(lax.all_to_all(own, far, 0, 0, tiled=True), axis=0)  20.4 us
    all_to_all x1, waiting for transfers between devices, sent_and_summed(): lax.all_to_all(cut_along(value, dim, length), axis, 0, 0, tiled=True)  10.8 us
    all_to_all x1, blocking collectives, sent_and_summed(): lax.all_to_all(cut_along(value, dim, length), axis, 0, 0, tiled=True)  8.24 us
    another operation x2, other arithmetic  7.61 us
    dot_general x1, matrix products, per_device(): lax.dot_general(attention_input, query_cotangent, contract, preferred_ele...  4.89 us
  transfers between devices with their start and end apart: 9, of which 8 were waited for; matrix products, arithmetic and copies ran while one was open for 9% of the time, Pallas kernels for 0%

commit v1 on v0

v1 whole, which is shorter than its diff:
```python
import jax
import jax.numpy as jnp
from jax import lax
from jax.sharding import Mesh
from jax.sharding import PartitionSpec as P

FS = ("zh", "zl", "yh", "yl")
NEAR = ("zl", "yl", "x")
FAR = ("zh", "yh")
PAIR = ("x", "c")

BETA_ONE = 0.9
BETA_TWO = 0.95
STEP_RATE = 0.01
EPSILON = 1e-08
NORM_FLOOR = 1e-06
BF = jnp.bfloat16
F32 = jnp.float32


def swap(pieces, axes):
    return lax.all_to_all(pieces, axes, 0, 0, tiled=True)


def rounded(v):
    return lax.reduce_precision(v, 8, 7)


def split_two(v):
    high = rounded(v)
    return high.astype(BF), (v - high).astype(BF)


def dot_two(a, b):
    high, low = split_two(b)
    return jnp.dot(a, high, preferred_element_type=F32) + jnp.dot(a, low, preferred_element_type=F32)


def per_device(
    attention_input,
    query_cotangent,
    gate_cotangent,
    gate_totals,
    projector,
    query_master,
    lowrank_mean,
    lowrank_square,
    gating_mean,
    gating_square,
):
    nz, ny, nzl, nyl, nx, nc = (lax.axis_size(a) for a in ("zh", "yh", "zl", "yl", "x", "c"))
    far, near = nz * ny, nzl * nyl * nx
    tokens, width = attention_input.shape
    columns = query_cotangent.shape[1]
    heads = gate_cotangent.shape[0]
    own, rank = projector.shape
    lanes = columns // nx
    block = rank // nx
    rows = block // far
    tokens_all = tokens * far * near
    norming = 1.0 / tokens_all**0.5
    contract = (((0,), (0,)), ((), ()))

    factor = swap(jnp.broadcast_to(projector[None], (far, own, rank)), FAR).reshape(far * own, rank)

    partial = lax.dot_general(attention_input, query_cotangent, contract, preferred_element_type=F32)
    partial = partial.astype(BF).reshape(nz, nzl, ny, nyl, own, nx, lanes)
    partial = partial.transpose(1, 3, 5, 0, 2, 4, 6).reshape(near, far * own, lanes)
    near_sum = jnp.sum(swap(partial, NEAR).astype(F32), axis=0)

    earlier = jnp.concatenate([jnp.zeros((heads, 1), F32), gate_totals[:, :-1]], axis=1)
    later = lax.broadcasted_iota(jnp.int32, (tokens, tokens), 0) >= lax.broadcasted_iota(
        jnp.int32, (tokens, tokens), 1
    )
    trailing = jnp.dot(
        gate_cotangent, later.astype(F32), precision=lax.Precision.HIGHEST, preferred_element_type=F32
    )
    gate_signal = (trailing * -jnp.expm1(gate_totals - earlier)).astype(BF)
    gate_partial = jnp.dot(gate_signal, attention_input, preferred_element_type=F32)

    rank_partial = lax.dot_general(factor, rounded(near_sum).astype(BF), contract, preferred_element_type=F32)
    rank_partial = rank_partial.reshape(nx, far, rows, lanes).transpose(1, 0, 2, 3).reshape(far, nx * rows, lanes)
    second = jnp.concatenate(
        [
            near_sum.astype(BF).reshape(far, own, lanes),
            rank_partial.astype(BF),
            gate_partial.astype(BF).reshape(heads, far, width // far).transpose(1, 0, 2),
        ],
        axis=1,
    )
    second = jnp.sum(swap(second, FAR).astype(F32), axis=0) * norming
    gradient, rank_part, gate_part = jnp.split(second, [own, own + nx * rows])

    third = jnp.concatenate(
        [
            rank_part.reshape(nx, rows, lanes),
            jnp.zeros((nx, 8 - rows, lanes), F32),
            jnp.broadcast_to(gate_part[None], (nx, *gate_part.shape)),
        ],
        axis=1,
    )
    third = jnp.broadcast_to(third[None], (nzl * nyl, *third.shape)).reshape(near, *third.shape[1:])
    third = jnp.sum(swap(third, NEAR).reshape(nzl * nyl, nx, -1, lanes), axis=0)
    fourth = jnp.concatenate(
        [third[:, :rows].reshape(nx * rows, lanes), jnp.sum(third[:, 8:], axis=0)], axis=0
    )
    fourth = swap(jnp.broadcast_to(fourth[None], (far, *fourth.shape)), FAR)
    projected = (
        fourth[:, : nx * rows].reshape(far, nx, rows, lanes).transpose(0, 2, 1, 3).reshape(block, columns)
    )
    forget_gradient = fourth[:, nx * rows :].transpose(1, 0, 2).reshape(heads, width)

    mean_after = BETA_ONE * lowrank_mean + (1.0 - BETA_ONE) * projected
    square_after = BETA_TWO * lowrank_square + (1.0 - BETA_TWO) * projected * projected
    direction = mean_after / (jnp.sqrt(square_after) + EPSILON)
    place = lax.axis_index("x")
    own_factor = lax.dynamic_slice_in_dim(projector, place * block, block, 1)
    lifted_direction = dot_two(own_factor, direction)
    lifted_projected = dot_two(own_factor, projected).reshape(own, nx, lanes)
    mine = lax.broadcasted_iota(jnp.int32, (1, nx, 1), 1) == place
    lifted_projected = lifted_projected - jnp.where(mine, gradient[:, None, :], 0.0)
    sums = jnp.stack([jnp.sum(direction * direction), jnp.sum(projected * projected)])
    first_part = rounded(sums)
    second_part = rounded(sums - first_part)
    third_part = rounded(sums - first_part - second_part)
    scalars = jnp.stack([first_part, second_part, third_part]).reshape(6, 1)
    scalars = jnp.broadcast_to(jnp.pad(scalars, ((0, 2), (0, 0))), (8, lanes))
    fifth = jnp.concatenate(
        [
            lifted_direction.reshape(own, nx, lanes).transpose(1, 0, 2).reshape(nx * own, lanes),
            lifted_projected.transpose(1, 0, 2).reshape(nx * own, lanes),
            scalars,
        ],
        axis=0,
    ).astype(BF)
    fifth = swap(jnp.broadcast_to(fifth[None], (nx * nc, *fifth.shape)), PAIR).reshape(nx, nc, -1, lanes)
    scalars = jnp.sum(fifth[:, :, 2 * nx * own :, 0].astype(F32), axis=(0, 1))
    direction_squares = scalars[0] + scalars[2] + scalars[4]
    projected_squares = scalars[1] + scalars[3] + scalars[5]
    balance = jnp.sqrt(direction_squares / (projected_squares + NORM_FLOOR))
    lifts = lax.dynamic_index_in_dim(fifth, lax.axis_index("c"), 1, False)[:, : 2 * nx * own]
    lifts = jnp.sum(lifts.astype(F32), axis=0).reshape(2, nx, own, lanes)
    query_update = lifts[0] - balance * lifts[1]
    query_update = query_update.transpose(1, 0, 2).reshape(own, columns)
    query_renewed = query_master - STEP_RATE * query_update
    query_copy = query_renewed.astype(BF)
    gating_average = BETA_ONE * gating_mean + (1.0 - BETA_ONE) * forget_gradient
    gating_energy = BETA_TWO * gating_square + (1.0 - BETA_TWO) * forget_gradient * forget_gradient
    gating_update = gating_average / (jnp.sqrt(gating_energy) + EPSILON)
    return (
        query_update,
        query_renewed,
        query_copy,
        mean_after,
        square_after,
        gating_update,
        gating_average,
        gating_energy,
    )


def solution(mesh):
    split = Mesh(
        mesh.devices.reshape(4, 2, 4, 2, mesh.shape["rep"], mesh.shape["tp"]),
        ("zh", "zl", "yh", "yl", "x", "c"),
    )
    in_specs = (
        P((*FS, "x"), None),
        P((*FS, "x"), "c"),
        P("c", (*FS, "x")),
        P("c", (*FS, "x")),
        P(FS, None),
        P(FS, "c"),
        P("x", "c"),
        P("x", "c"),
        P("c", None),
        P("c", None),
    )
    out_specs = (
        P(FS, "c"),
        P(FS, "c"),
        P(FS, "c"),
        P("x", "c"),
        P("x", "c"),
        P("c", None),
        P("c", None),
        P("c", None),
    )
    return jax.shard_map(
        per_device, mesh=split, in_specs=in_specs, out_specs=out_specs, check_vma=False
    )
```

time: 238 us -> 156 us (0.66)
  waiting for transfers between devices: 108 us -> 42.1 us
  blocking collectives: 28.7 us -> 44.3 us
  starting transfers between devices: 43.4 us -> 32 us
  between operations: 15.5 us -> 4.77 us
  other arithmetic: 17.8 us -> 8.77 us
    reduce_scatter x2 -> x0, waiting for transfers between devices: 64.3 us -> none  [sum_by_axis_2(): running = lax.psum_scatter(running, axis, scatter_dimension=0, tiled=True)]
    all_to_all x2, blocking collectives: 28.7 us -> 44.3 us  [swap(): return lax.all_to_all(pieces, axes, 0, 0, tiled=True)]
    all_to_all x7 -> x4, starting transfers between devices: 43.3 us -> 32 us  [swap(): return lax.all_to_all(pieces, axes, 0, 0, tiled=True)]
    another operation x2, other arithmetic: 7.61 us -> 0.09 us
    reshape x1 -> x5, local copies, waits for them, and re-layouts: 0.79 us -> 6.21 us  [the longest x2 6.08 us: per_device(): partial = partial.astype(BF).reshape(nz, nzl, ny, nyl, own, nx, lanes)]
    mul x4 -> x0, local copies, waits for them, and re-layouts: 4.21 us -> none  [the longest x2 2.41 us: per_device(): gating_average = BETA_ONE * gating_mean + (1.0 - BETA_ONE) * forget_gradient]
    all_to_all x7 -> x4, waiting for transfers between devices: 44.2 us -> 42.1 us  [swap(): return lax.all_to_all(pieces, axes, 0, 0, tiled=True)]
  transfers between devices with their start and end apart: 9 -> 4, of which waited for: 8 -> 4; matrix products, arithmetic and copies ran while one was open for 9% -> 2% of each run, Pallas kernels for 0% -> 0%
where the time goes in v1:
time: 156 us; the launch traced here: 155 us
  blocking collectives  44.3 us (28%)
  waiting for transfers between devices  42.1 us (27%)
  starting transfers between devices  32 us (21%)
  local copies, waits for them, and re-layouts  14.7 us (9%)
  other arithmetic  8.77 us (6%)
  matrix products  8.51 us (5%)
  between operations  4.77 us (3%)
    all_to_all x2, blocking collectives, swap(): return lax.all_to_all(pieces, axes, 0, 0, tiled=True)  44.3 us
    all_to_all x4, waiting for transfers between devices, swap(): return lax.all_to_all(pieces, axes, 0, 0, tiled=True)  42.1 us
    all_to_all x4, starting transfers between devices, swap(): return lax.all_to_all(pieces, axes, 0, 0, tiled=True)  32 us
    reshape x2, local copies, waits for them, and re-layouts, per_device(): partial = partial.astype(BF).reshape(nz, nzl, ny, nyl, own, nx, lanes)  6.08 us
    dot_general x1, matrix products, per_device(): lax.dot_general(attention_input, query_cotangent, contract, preferred_ele...  4.32 us
  transfers between devices with their start and end apart: 4, of which 4 were waited for; matrix products, arithmetic and copies ran while one was open for 2% of the time, Pallas kernels for 0%

profile of v1, /device:TPU:1, one launch (start us, length us, event | category | flops | bytes accessed | tf_op | source)
XLA Modules:
  0.0 155.1 jit_solution(247134982415972586)
XLA Ops:
  0.6 0.0 copy-start
  0.6 1.9 %copy-done = bf16[768,2048]{1,0:T(8,128)(2,1)S(1)} copy-done((bf16[768,2048]{1,0:T(8,128)(2,1)S(1)}, bf16[768,2048]{1,0:T(8,128)(2,1)}, u32[]{:S(2)}) %copy-start) | copy-done | bytes 3145752
  2.5 4.3 %convolution_convert_fusion = bf16[2048,512]{1,0:T(8,128)(2,1)} fusion(bf16[768,2048]{1,0:T(8,128)(2,1)S(1)} %copy-done, bf16[768,512]{1,0:T(8,128)(2,1)} %param.11), kind=kOutput, calls=%fused_computation.1 | convolution fusion | flops 1611661312 | bytes 6029312 | tf_op jit(solution)/shard_map/dot_general | solution.py:66
  6.8 4.0 %reshape.243 = bf16[4,2,4,2,32,4,128]{6,5,4,3,2,1,0:T(4,128)(2,1)} reshape(bf16[2048,512]{1,0:T(8,128)(2,1)} %convolution_convert_fusion) | data formatting | bytes 4194304 | tf_op jit(solution)/shard_map/reshape | solution.py:67
  10.8 2.1 %copy.51 = bf16[4,2,4,2,32,4,128]{6,4,2,0,5,3,1:T(8,128)(2,1)S(1)} copy(bf16[4,2,4,2,32,4,128]{6,5,4,3,2,1,0:T(4,128)(2,1)} %reshape.243) | data formatting | bytes 4194304 | tf_op jit(solution)/shard_map/reshape | solution.py:67
  12.9 0.0 copy-start.3
  12.9 0.0 copy-start.6
  13.0 0.0 copy-start.7
  13.0 34.3 %all_to_all.30 = bf16[16,512,128]{2,1,0:T(8,128)(2,1)} all-to-all(bf16[16,512,128]{2,1,0:T(8,128)(2,1)S(1)} %bitcast.92), channel_id=1, replica_groups=mesh['zh'=4,'zl'=2,'yh'=4,'yl'=2,'x'=4,'c'=2] {'zl','yl','x'}, dimensions={0} | all-to-all | bytes 4194304 | tf_op jit(solution)/shard_map/all_to_all | solution.py:22
  47.3 0.7 broadcast_in_dim.32
  48.0 14.5 %all-to-all-start.1 = ((bf16[16,32,256]{2,1,0:T(8,128)(2,1)}), bf16[16,32,256]{2,1,0:T(8,128)(2,1)}, u32[]{:S(2)}, u32[]{:S(2)}) async-start(bf16[16,32,256]{2,1,0:T(8,128)(2,1)} %broadcast_in_dim.32), calls=%async_computation.1 | async-start | bytes 524288 | tf_op jit(solution)/shard_map/all_to_all | solution.py:22
  62.5 0.4 fusion.8
  63.0 1.1 fusion.5
  64.1 0.3 convert_reduce_fusion
  64.4 10.5 %all-to-all-done.1 = bf16[16,32,256]{2,1,0:T(8,128)(2,1)} async-done(((bf16[16,32,256]{2,1,0:T(8,128)(2,1)}), bf16[16,32,256]{2,1,0:T(8,128)(2,1)}, u32[]{:S(2)}, u32[]{:S(2)}) %all-to-all-start.1) | async-done | bytes 262176 | tf_op jit(solution)/shard_map/all_to_all | solution.py:22
  75.0 1.8 %fusion.2 = bf16[256,128]{0,1:T(8,128)(2,1)} fusion(bf16[512,256]{1,0:T(8,128)(2,1)} %bitcast.3, f32[512,128]{1,0:T(8,128)S(1)} %convert_reduce_fusion), kind=kOutput, calls=%fused_computation.9 | convolution fusion | flops 33718272 | bytes 589824 | tf_op jit(solution)/shard_map/dot_general | solution.py:81
  76.8 0.9 copy.52
  77.8 1.5 pad_maximum_fusion
  79.2 4.4 %all-to-all-start.2 = ((bf16[16,56,128]{2,1,0:T(8,128)(2,1)}), bf16[16,56,128]{2,1,0:T(8,128)(2,1)S(1)}, u32[]{:S(2)}, u32[]{:S(2)}) async-start(bf16[16,56,128]{2,1,0:T(8,128)(2,1)} %pad_maximum_fusion), calls=%async_computation.2 | async-start | bytes 458752 | tf_op jit(solution)/shard_map/all_to_all | solution.py:22
  83.7 0.0 copy-start.4
  83.7 0.1 pad.20.clone
  83.7 11.9 %all-to-all-done.2 = bf16[16,56,128]{2,1,0:T(8,128)(2,1)S(1)} async-done(((bf16[16,56,128]{2,1,0:T(8,128)(2,1)}), bf16[16,56,128]{2,1,0:T(8,128)(2,1)S(1)}, u32[]{:S(2)}, u32[]{:S(2)}) %all-to-all-start.2) | async-done | bytes 229408 | tf_op jit(solution)/shard_map/all_to_all | solution.py:22
  95.7 0.1 pad_maximum_fusion.1
  95.8 9.9 %all_to_all.31 = f32[16,16,128]{2,1,0:T(8,128)S(1)} all-to-all(f32[16,16,128]{2,1,0:T(8,128)S(1)} %bitcast.100), channel_id=1, replica_groups=mesh['zh'=4,'zl'=2,'yh'=4,'yl'=2,'x'=4,'c'=2] {'zl','yl','x'}, dimensions={0} | all-to-all | bytes 262144 | tf_op jit(solution)/shard_map/all_to_all | solution.py:22
  105.8 0.7 broadcast_in_dim.36
  106.5 5.9 %all-to-all-start.4 = ((f32[16,24,128]{2,1,0:T(8,128)}), f32[16,24,128]{2,1,0:T(8,128)S(1)}, u32[]{:S(2)}, u32[]{:S(2)}) async-start(f32[16,24,128]{2,1,0:T(8,128)} %broadcast_in_dim.36), calls=%async_computation.4 | async-start | bytes 393216 | tf_op jit(solution)/shard_map/all_to_all | solution.py:22
  112.4 11.5 %all-to-all-done.4 = f32[16,24,128]{2,1,0:T(8,128)S(1)} async-done(((f32[16,24,128]{2,1,0:T(8,128)}), f32[16,24,128]{2,1,0:T(8,128)S(1)}, u32[]{:S(2)}, u32[]{:S(2)}) %all-to-all-start.4) | async-done | bytes 196640 | tf_op jit(solution)/shard_map/all_to_all | solution.py:22
  123.9 0.7 copy-done.2
  124.6 0.7 fusion.13
  125.3 2.3 %multiply_reduce_fusion = (f32[]{:T(128)}, f32[64,512]{1,0:T(8,128)S(1)}, f32[64,512]{1,0:T(8,128)}, f32[64,512]{1,0:T(8,128)}) fusion(f32[8,8,4,128]{3,2,1,0:T(4,128)S(1)} %bitcast.93, f32[64,512]{1,0:T(8,128)} %param.17, f32[64,512]{1,0:T(8,128)} %param.16), kind=kLoop, calls=%fused_computation.33 | loop fusion | flops 360447 | bytes 786436 | tf_op jit(solution)/shard_map/reduce_sum | solution.py:122
  127.7 1.4 fusion.31
  129.0 0.1 reshape.255
  129.1 0.2 fusion.18
  129.3 0.2 fusion.17
  129.5 0.2 fusion.4
  129.7 0.0 copy-start.5
  129.8 0.2 fusion.1
  130.0 0.1 fusion.19
  130.1 0.1 maximum_maximum_fusion
  130.2 0.9 broadcast_in_dim.65
  131.0 7.2 %all-to-all-start.5 = ((bf16[8,264,128]{2,1,0:T(8,128)(2,1)}), bf16[8,264,128]{2,1,0:T(8,128)(2,1)}, u32[]{:S(2)}, u32[]{:S(2)}) async-start(bf16[8,264,128]{2,1,0:T(8,128)(2,1)} %broadcast_in_dim.65), calls=%async_computation.5 | async-start | bytes 1081344 | tf_op jit(solution)/shard_map/all_to_all | solution.py:22
  138.3 1.6 %add_divide_fusion.1 = (f32[8,2048]{1,0:T(8,128)}, f32[8,2048]{1,0:T(8,128)}, f32[8,2048]{1,0:T(8,128)}) fusion(f32[16,24,128]{2,1,0:T(8,128)} %copy-done.2, f32[8,2048]{1,0:T(8,128)S(1)} %copy-done.4, f32[8,2048]{1,0:T(8,128)} %param.18), kind=kLoop, calls=%fused_computation.46 | loop fusion | flops 147456 | bytes 393216 | tf_op jit(solution)/shard_map/div | solution.py:149
  139.8 8.1 %all-to-all-done.5 = bf16[8,264,128]{2,1,0:T(8,128)(2,1)} async-done(((bf16[8,264,128]{2,1,0:T(8,128)(2,1)}), bf16[8,264,128]{2,1,0:T(8,128)(2,1)}, u32[]{:S(2)}, u32[]{:S(2)}) %all-to-all-start.5) | async-done | bytes 540704 | tf_op jit(solution)/shard_map/all_to_all | solution.py:22
  147.9 0.7 slice.67
  148.7 0.1 copy.60
  148.8 0.7 fusion.34
  153.3 1.0 dynamic-slice_bitcast_fusion
  154.4 0.7 fusion.30
  (34 shorter events, 0.3 us)
Async XLA Ops:
  0.6 1.9 %copy-start = (bf16[768,2048]{1,0:T(8,128)(2,1)S(1)}, bf16[768,2048]{1,0:T(8,128)(2,1)}, u32[]{:S(2)}) copy-start(bf16[768,2048]{1,0:T(8,128)(2,1)} %param.10) | copy-start | bytes 9437188
  12.9 34.4 %copy-start.3 = (bf16[32,256]{1,0:T(8,128)(2,1)S(1)}, bf16[32,256]{1,0:T(8,128)(2,1)}, u32[]{:S(2)}) copy-start(bf16[32,256]{1,0:T(8,128)(2,1)} %param.14) | copy-start | bytes 49156
  12.9 49.6 %copy-start.6 = (f32[8,768]{1,0:T(8,128)S(1)}, f32[8,768]{1,0:T(8,128)}, u32[]{:S(2)}) copy-start(f32[8,768]{1,0:T(8,128)} %param.12) | copy-start | bytes 73732
  13.0 49.6 %copy-start.7 = (f32[8,768]{1,0:T(8,128)S(1)}, f32[8,768]{1,0:T(8,128)}, u32[]{:S(2)}) copy-start(f32[8,768]{1,0:T(8,128)} %param.13) | copy-start | bytes 73732
  48.0 26.9 %all-to-all-start.1 = ((bf16[16,32,256]{2,1,0:T(8,128)(2,1)}), bf16[16,32,256]{2,1,0:T(8,128)(2,1)}, u32[]{:S(2)}, u32[]{:S(2)}) async-start(bf16[16,32,256]{2,1,0:T(8,128)(2,1)} %broadcast_in_dim.32), calls=%async_computation.1 | async-start | bytes 524288 | tf_op jit(solution)/shard_map/all_to_all | solution.py:22
  62.5 1.6 %copy-start.1 = (bf16[16,512,128]{2,1,0:T(8,128)(2,1)S(1)}, bf16[16,512,128]{2,1,0:T(8,128)(2,1)}, u32[]{:S(2)}) copy-start(bf16[16,512,128]{2,1,0:T(8,128)(2,1)} %all_to_all.30) | copy-start | bytes 6291460
  79.2 16.4 %all-to-all-start.2 = ((bf16[16,56,128]{2,1,0:T(8,128)(2,1)}), bf16[16,56,128]{2,1,0:T(8,128)(2,1)S(1)}, u32[]{:S(2)}, u32[]{:S(2)}) async-start(bf16[16,56,128]{2,1,0:T(8,128)(2,1)} %pad_maximum_fusion), calls=%async_computation.2 | async-start | bytes 458752 | tf_op jit(solution)/shard_map/all_to_all | solution.py:22
  83.7 54.6 %copy-start.4 = (f32[8,2048]{1,0:T(8,128)S(1)}, f32[8,2048]{1,0:T(8,128)}, u32[]{:S(2)}) copy-start(f32[8,2048]{1,0:T(8,128)} %param.19) | copy-start | bytes 196612
  106.5 17.4 %all-to-all-start.4 = ((f32[16,24,128]{2,1,0:T(8,128)}), f32[16,24,128]{2,1,0:T(8,128)S(1)}, u32[]{:S(2)}, u32[]{:S(2)}) async-start(f32[16,24,128]{2,1,0:T(8,128)} %broadcast_in_dim.36), calls=%async_computation.4 | async-start | bytes 393216 | tf_op jit(solution)/shard_map/all_to_all | solution.py:22
  123.9 0.7 copy-start.2
  129.7 24.7 %copy-start.5 = (f32[32,512]{1,0:T(8,128)S(1)}, f32[32,512]{1,0:T(8,128)}, u32[]{:S(2)}) copy-start(f32[32,512]{1,0:T(8,128)} %param.15) | copy-start | bytes 196612
  131.0 16.9 %all-to-all-start.5 = ((bf16[8,264,128]{2,1,0:T(8,128)(2,1)}), bf16[8,264,128]{2,1,0:T(8,128)(2,1)}, u32[]{:S(2)}, u32[]{:S(2)}) async-start(bf16[8,264,128]{2,1,0:T(8,128)(2,1)} %broadcast_in_dim.65), calls=%async_computation.5 | async-start | bytes 1081344 | tf_op jit(solution)/shard_map/all_to_all | solution.py:22

commit v2 on v1

v2 whole, which is shorter than its diff:
```python
import functools

import jax
import jax.numpy as jnp
from jax import lax
from jax.experimental import pallas as pl
from jax.experimental.pallas import tpu as pltpu
from jax.sharding import Mesh
from jax.sharding import PartitionSpec as P

FS = ("zh", "zl", "yh", "yl")
NEAR = ("zl", "yl", "x")
FAR = ("zh", "yh")
PAIR = ("x", "c")

BETA_ONE = 0.9
BETA_TWO = 0.95
STEP_RATE = 0.01
EPSILON = 1e-08
NORM_FLOOR = 1e-06
BF = jnp.bfloat16
F32 = jnp.float32
FIRST = (((0,), (0,)), ((), ()))
LANES = 128
VMEM = pl.BlockSpec(memory_space=pltpu.VMEM)
SMEM = pl.BlockSpec(memory_space=pltpu.SMEM)


def swap(pieces, axes):
    return lax.all_to_all(pieces, axes, 0, 0, tiled=True)


def shifted(value, axis, step):
    length = lax.axis_size(axis)
    return lax.ppermute(value, axis, [(i, (i + step) % length) for i in range(length)])


def turned(value, axis):
    steps = range(1, lax.axis_size(axis))
    return jnp.stack([value, *(shifted(value, axis, s) for s in steps)])


def split_two(v):
    high = v.astype(BF)
    return high, (v - high.astype(F32)).astype(BF)


def dot(a, b, dims=(((1,), (0,)), ((), ()))):
    return lax.dot_general(a, b, dims, preferred_element_type=F32)


def one_less_exp(v):
    series = 1.0 + v * 0.125
    for k in range(7, 1, -1):
        series = 1.0 + v * (1.0 / k) * series
    return jnp.where(v > -0.3, -v * series, 1.0 - jnp.exp(v))


def first_kernel(sizes, x_ref, q_ref, cot_ref, tot_ref, out_ref, signal):
    nzl, ny, nyl, nx, own = sizes
    step = pl.program_id(0)

    @pl.when(step == 0)
    def _():
        cot = cot_ref[...]
        heads, tokens = cot.shape
        later = lax.broadcasted_iota(jnp.int32, (tokens, tokens), 0) >= lax.broadcasted_iota(
            jnp.int32, (tokens, tokens), 1
        )
        later = jnp.where(later, 1.0, 0.0).astype(BF)
        one = cot.astype(BF)
        rest = cot - one.astype(F32)
        two = rest.astype(BF)
        three = (rest - two.astype(F32)).astype(BF)
        trailing = dot(three, later) + dot(two, later) + dot(one, later)
        totals = tot_ref[...]
        earlier = pltpu.roll(totals, 1, 1)
        lane = lax.broadcasted_iota(jnp.int32, totals.shape, 1)
        gate = totals - jnp.where(lane == 0, 0.0, earlier)
        signal[...] = (trailing * one_less_exp(gate)).astype(BF)

    block = x_ref[...]
    part = dot(block, q_ref[...], FIRST).astype(BF)
    zh, zl = step // nzl, lax.rem(step, nzl)
    for yh in range(ny):
        for yl in range(nyl):
            row = (yh * nyl + yl) * own
            for q in range(nx):
                out_ref[(zl * nyl + yl) * nx + q, pl.ds((zh * ny + yh) * own, own), :] = part[
                    row : row + own, q * LANES : (q + 1) * LANES
                ]
    gates = dot(signal[...], block).astype(BF)
    far_rows = out_ref.shape[1] - gates.shape[0]
    per_step = gates.shape[1] // LANES
    for k in range(per_step):
        out_ref[step * per_step + k, far_rows:, :] = gates[:, k * LANES : (k + 1) * LANES]


def second_kernel(sizes, at_ref, p_ref, in_ref, out_ref, total):
    nz, ny, own, rank_rows, heads = sizes
    summed = in_ref[0].astype(F32)
    for k in range(1, in_ref.shape[0]):
        summed = summed + in_ref[k].astype(F32)
    total[...] = summed
    rows = nz * ny * own
    rank = None
    for b in range(ny):
        for a in range(nz):
            zh = lax.rem(at_ref[0] + nz - a, nz)
            yh = lax.rem(at_ref[1] + ny - b, ny)
            high, low = split_two(total[pl.ds((zh * ny + yh) * own, own), :])
            factor = p_ref[b, a]
            term = dot(factor, high, FIRST) + dot(factor, low, FIRST)
            rank = term if rank is None else rank + term
    gates = total[rows:, :].astype(BF)
    for k in range(nz * ny):
        out_ref[k, :own, :] = total[k * own : (k + 1) * own, :].astype(BF)
        high, low = split_two(rank[k * rank_rows : (k + 1) * rank_rows, :])
        out_ref[k, own : own + rank_rows, :] = high
        out_ref[k, own + rank_rows : own + 2 * rank_rows, :] = low
        out_ref[k, own + 2 * rank_rows :, :] = gates


def third_kernel(sizes, norming, in_ref, gradient_ref, out_ref, gate_ref):
    own, rank_rows = sizes
    summed = in_ref[0].astype(F32)
    for k in range(1, in_ref.shape[0]):
        summed = summed + in_ref[k].astype(F32)
    summed = summed * norming
    gradient_ref[...] = summed[:own]
    rank = (summed[own : own + rank_rows] + summed[own + rank_rows : own + 2 * rank_rows]).astype(BF)
    for k in range(out_ref.shape[0]):
        out_ref[k] = rank
    gate_ref[...] = summed[own + 2 * rank_rows :]


def fourth_kernel(sizes, at_ref, in_ref, moments_ref, p_ref, gradient_ref, out_ref, projected, direction):
    nz, nzl, ny, nyl, nx, nc, rank_rows = sizes
    for zh in range(nz):
        for yh in range(ny):
            piece = None
            for zl in range(nzl):
                for yl in range(nyl):
                    term = in_ref[((zh * nzl + zl) * ny + yh) * nyl + yl].astype(F32)
                    piece = term if piece is None else piece + term
            k = zh * ny + yh
            projected[k * rank_rows : (k + 1) * rank_rows, :] = piece
    block = projected.shape[0] // nx
    squares = jnp.zeros((2, LANES), F32)
    for s in range(nx):
        where = lax.rem(at_ref[2] + nx - s, nx) * block
        p = projected[pl.ds(where, block), :]
        mean = BETA_ONE * moments_ref[s, :block] + (1.0 - BETA_ONE) * p
        square = BETA_TWO * moments_ref[s, block:] + (1.0 - BETA_TWO) * p * p
        d = mean / (jnp.sqrt(square) + EPSILON)
        direction[pl.ds(where, block), :] = d
        squares = squares + jnp.concatenate(
            [jnp.sum(d * d, axis=0, keepdims=True), jnp.sum(p * p, axis=0, keepdims=True)], axis=0
        )
    factor = p_ref[...]
    own = factor.shape[0]
    high, low = split_two(direction[...])
    lifted_direction = dot(factor, high) + dot(factor, low)
    high, low = split_two(projected[...])
    lifted_projected = dot(factor, high) + dot(factor, low) - gradient_ref[...]
    squares = jnp.concatenate([squares, jnp.zeros((6, LANES), F32)], axis=0)
    for x in range(nx):
        for c in range(nc):
            k = x * nc + c
            out_ref[k, :own] = lifted_direction
            out_ref[k, own : 2 * own] = lifted_projected
            out_ref[k, 2 * own : 2 * own + block] = projected[x * block : (x + 1) * block, :]
            out_ref[k, 2 * own + block :] = squares


def last_kernel(
    sizes, at_ref, in_ref, master_ref, mean_ref, square_ref, update_ref, new_ref, copy_ref, mean_out, square_out
):
    nx, nc, own, block = sizes
    squares = in_ref[0, 2 * own + block :]
    for k in range(1, nx * nc):
        squares = squares + in_ref[k, 2 * own + block :]
    direction_squares = jnp.sum(squares[0:1], axis=1, keepdims=True)
    projected_squares = jnp.sum(squares[1:2], axis=1, keepdims=True)
    balance = jnp.sqrt(direction_squares / (projected_squares + NORM_FLOOR))
    for x in range(nx):
        k = x * nc + at_ref[3]
        cut = slice(x * LANES, (x + 1) * LANES)
        update = in_ref[k, :own] - balance * in_ref[k, own : 2 * own]
        update_ref[:, cut] = update
        new = master_ref[:, cut] - STEP_RATE * update
        new_ref[:, cut] = new
        copy_ref[:, cut] = new.astype(BF)
        p = in_ref[k, 2 * own : 2 * own + block]
        mean_out[:, cut] = BETA_ONE * mean_ref[:, cut] + (1.0 - BETA_ONE) * p
        square_out[:, cut] = BETA_TWO * square_ref[:, cut] + (1.0 - BETA_TWO) * p * p


def gate_kernel(sizes, at_ref, in_ref, mean_ref, square_ref, update_ref, average_ref, energy_ref):
    nzl, nyl, nx = sizes
    for a in range(nzl):
        for b in range(nyl):
            for s in range(nx):
                zl = lax.rem(at_ref[4] + nzl - a, nzl)
                yl = lax.rem(at_ref[5] + nyl - b, nyl)
                x = lax.rem(at_ref[2] + nx - s, nx)
                cut = pl.ds(((zl * nyl + yl) * nx + x) * LANES, LANES)
                g = in_ref[a, b, s]
                average = BETA_ONE * mean_ref[:, cut] + (1.0 - BETA_ONE) * g
                energy = BETA_TWO * square_ref[:, cut] + (1.0 - BETA_TWO) * g * g
                average_ref[:, cut] = average
                energy_ref[:, cut] = energy
                update_ref[:, cut] = average / (jnp.sqrt(energy) + EPSILON)


def per_device(
    attention_input,
    query_cotangent,
    gate_cotangent,
    gate_totals,
    projector,
    query_master,
    lowrank_mean,
    lowrank_square,
    gating_mean,
    gating_square,
):
    nz, ny, nzl, nyl, nx, nc = (lax.axis_size(a) for a in ("zh", "yh", "zl", "yl", "x", "c"))
    far, near = nz * ny, nzl * nyl * nx
    tokens, width = attention_input.shape
    columns = query_cotangent.shape[1]
    heads = gate_cotangent.shape[0]
    own, rank = projector.shape
    block = rank // nx
    rank_rows = rank // far
    norming = 1.0 / (tokens * far * near) ** 0.5
    shape = jax.ShapeDtypeStruct
    at = jnp.stack([lax.axis_index(a) for a in ("zh", "yh", "x", "c", "zl", "yl")]).astype(jnp.int32)

    factors = turned(turned(projector, "zh"), "yh")

    cut = ny * nyl * own
    first = pl.pallas_call(
        functools.partial(first_kernel, (nzl, ny, nyl, nx, own)),
        out_shape=shape((near, far * own + heads, LANES), BF),
        grid=(nz * nzl,),
        in_specs=[
            pl.BlockSpec((tokens, cut), lambda z: (0, z)),
            pl.BlockSpec((tokens, columns), lambda z: (0, 0)),
            pl.BlockSpec((heads, tokens), lambda z: (0, 0)),
            pl.BlockSpec((heads, tokens), lambda z: (0, 0)),
        ],
        out_specs=pl.BlockSpec((near, far * own + heads, LANES), lambda z: (0, 0, 0)),
        scratch_shapes=[pltpu.VMEM((heads, tokens), BF)],
        name="first",
    )(attention_input, query_cotangent, gate_cotangent, gate_totals)
    first = swap(first, NEAR)

    mine = jnp.concatenate(
        [lowrank_mean.reshape(block, nx, LANES), lowrank_square.reshape(block, nx, LANES)]
    ).transpose(1, 0, 2)
    first, mine = lax.optimization_barrier((first, mine))
    second = pl.pallas_call(
        functools.partial(second_kernel, (nz, ny, own, rank_rows, heads)),
        out_shape=shape((far, own + 2 * rank_rows + heads, LANES), BF),
        in_specs=[SMEM, VMEM, VMEM],
        out_specs=VMEM,
        scratch_shapes=[pltpu.VMEM((far * own + heads, LANES), F32)],
        name="second",
    )(at, factors, first)
    second = swap(second, FAR)

    moments = [lax.dynamic_index_in_dim(mine, at[2], 0, False)]
    for s in range(1, nx):
        piece = lax.dynamic_index_in_dim(mine, lax.rem(at[2] + s, nx), 0, False)
        moments.append(shifted(piece, "x", s))
    moments = jnp.stack(moments)
    second, moments = lax.optimization_barrier((second, moments))

    gradient, third, gates = pl.pallas_call(
        functools.partial(third_kernel, (own, rank_rows), norming),
        out_shape=(
            shape((own, LANES), F32),
            shape((far * nzl * nyl, rank_rows, LANES), BF),
            shape((heads, LANES), F32),
        ),
        in_specs=[VMEM],
        out_specs=(VMEM, VMEM, VMEM),
        name="third",
    )(second)
    third = swap(third, FS)
    gates = turned(turned(turned(gates, "x"), "yl"), "zl")
    third, gates = lax.optimization_barrier((third, gates))

    fourth = pl.pallas_call(
        functools.partial(fourth_kernel, (nz, nzl, ny, nyl, nx, nc, rank_rows)),
        out_shape=shape((nx * nc, 2 * own + block + 8, LANES), F32),
        in_specs=[SMEM, VMEM, VMEM, VMEM, VMEM],
        out_specs=VMEM,
        scratch_shapes=[pltpu.VMEM((rank, LANES), F32), pltpu.VMEM((rank, LANES), F32)],
        name="fourth",
    )(at, third, moments, projector, gradient)
    fourth = swap(fourth, PAIR)

    gating_update, gating_average, gating_energy = pl.pallas_call(
        functools.partial(gate_kernel, (nzl, nyl, nx)),
        out_shape=(shape((heads, width), F32),) * 3,
        in_specs=[SMEM, VMEM, VMEM, VMEM],
        out_specs=(VMEM,) * 3,
        name="gating",
    )(at, gates, gating_mean, gating_square)

    query_update, query_renewed, query_copy, mean_after, square_after = pl.pallas_call(
        functools.partial(last_kernel, (nx, nc, own, block)),
        out_shape=(
            shape((own, columns), F32),
            shape((own, columns), F32),
            shape((own, columns), BF),
            shape((block, columns), F32),
            shape((block, columns), F32),
        ),
        in_specs=[SMEM, VMEM, VMEM, VMEM, VMEM],
        out_specs=(VMEM,) * 5,
        name="last",
    )(at, fourth, query_master, lowrank_mean, lowrank_square)
    return (
        query_update,
        query_renewed,
        query_copy,
        mean_after,
        square_after,
        gating_update,
        gating_average,
        gating_energy,
    )


def solution(mesh):
    split = Mesh(
        mesh.devices.reshape(4, 2, 4, 2, mesh.shape["rep"], mesh.shape["tp"]),
        ("zh", "zl", "yh", "yl", "x", "c"),
    )
    in_specs = (
        P((*FS, "x"), None),
        P((*FS, "x"), "c"),
        P("c", (*FS, "x")),
        P("c", (*FS, "x")),
        P(FS, None),
        P(FS, "c"),
        P("x", "c"),
        P("x", "c"),
        P("c", None),
        P("c", None),
    )
    out_specs = (
        P(FS, "c"),
        P(FS, "c"),
        P(FS, "c"),
        P("x", "c"),
        P("x", "c"),
        P("c", None),
        P("c", None),
        P("c", None),
    )
    return jax.shard_map(
        per_device, mesh=split, in_specs=in_specs, out_specs=out_specs, check_vma=False
    )
```

time: 156 us -> 160 us (1.026)
  starting transfers between devices: 32 us -> 89.8 us
  blocking collectives: 44.3 us -> 0 us
  Pallas kernels: 0 us -> 19.5 us
  local copies, waits for them, and re-layouts: 14.7 us -> 4.29 us
  matrix products: 8.51 us -> 0 us
  other arithmetic: 8.77 us -> 2.84 us
  between operations: 4.77 us -> 0.89 us
    ppermute x0 -> x14, starting transfers between devices: none -> 51.1 us  [shifted(): lax.ppermute(value, axis, [(i, (i + step) % length) for i in range(length)])]
    all_to_all x2 -> x0, blocking collectives: 44.3 us -> none  [swap(): return lax.all_to_all(pieces, axes, 0, 0, tiled=True)]
    all_to_all x4, waiting for transfers between devices: 42.1 us -> 8.08 us  [swap(): return lax.all_to_all(pieces, axes, 0, 0, tiled=True)]
    ppermute x0 -> x14, waiting for transfers between devices: none -> 33.1 us  [shifted(): lax.ppermute(value, axis, [(i, (i + step) % length) for i in range(length)])]
    pallas_call x0 -> x6, Pallas kernels: none -> 19.5 us  [the longest x1 8.49 us: per_device(): pl.pallas_call(functools.partial(first_kernel, (nzl, ny, nyl, nx, own)),...]
    dot_general x8 -> x0, matrix products: 8.51 us -> none  [the longest x1 4.32 us: per_device(): lax.dot_general(attention_input, query_cotangent, contract, preferred_ele...]
    all_to_all x4, starting transfers between devices: 32 us -> 38.7 us  [swap(): return lax.all_to_all(pieces, axes, 0, 0, tiled=True)]
    reshape x5 -> x1, local copies, waits for them, and re-layouts: 6.21 us -> 0.02 us  [per_device(): lowrank_square.reshape(block, nx, LANES)]
  transfers between devices with their start and end apart: 4 -> 18, of which waited for: 4 -> 10; matrix products, arithmetic and copies ran while one was open for 2% -> 2% of each run, Pallas kernels for 0% -> 1%
where the time goes in v2:
time: 160 us; the launch traced here: 158 us
  starting transfers between devices  89.8 us (56%)
  waiting for transfers between devices  41.1 us (26%)
  Pallas kernels  19.5 us (12%)
  local copies, waits for them, and re-layouts  4.29 us (3%)
  other arithmetic  2.84 us (2%)
    ppermute x14, starting transfers between devices, shifted(): lax.ppermute(value, axis, [(i, (i + step) % length) for i in range(length)])  51.1 us
    all_to_all x4, starting transfers between devices, swap(): return lax.all_to_all(pieces, axes, 0, 0, tiled=True)  38.7 us
    ppermute x14, waiting for transfers between devices, shifted(): lax.ppermute(value, axis, [(i, (i + step) % length) for i in range(length)])  33.1 us
    pallas_call x1, Pallas kernels, per_device(): pl.pallas_call(functools.partial(first_kernel, (nzl, ny, nyl, nx, own)),...  8.49 us
    all_to_all x4, waiting for transfers between devices, swap(): return lax.all_to_all(pieces, axes, 0, 0, tiled=True)  8.08 us
    unnamed x14, local copies, waits for them, and re-layouts  3.62 us
    pallas_call x1, Pallas kernels, per_device(): pl.pallas_call(functools.partial(second_kernel, (nz, ny, own, rank_rows,...  3.49 us
  transfers between devices with their start and end apart: 18, of which 10 were waited for; matrix products, arithmetic and copies ran while one was open for 2% of the time, Pallas kernels for 1%

profile of v2, /device:TPU:1, one launch (start us, length us, event | category | flops | bytes accessed | tf_op | source)
XLA Modules:
  0.0 158.5 jit_solution(10224393003389741256)
XLA Ops:
  0.6 8.5 %first.1 = bf16[16,520,128]{2,1,0:T(8,128)(2,1)} custom-call(bf16[768,2048]{1,0:T(8,128)(2,1)} %x_ref.1, bf16[768,512]{1,0:T(8,128)(2,1)} %q_ref.1, f32[8,768]{1,0:T(8,128)} %cot_ref.1, f32[8,768]{1,0:T(8,128)} %tot_ref.1), custom_call_target="tpu_custom_call" | custom-call | tf_op jit(solution)/shard_map/first/pallas_call | solution.py:243
  9.1 7.9 %all-to-all-start = ((bf16[16,520,128]{2,1,0:T(8,128)(2,1)}), bf16[16,520,128]{2,1,0:T(8,128)(2,1)S(1)}, u32[]{:S(2)}, u32[]{:S(2)}) async-start(bf16[16,520,128]{2,1,0:T(8,128)(2,1)} %first.1), calls=%async_computation | async-start | bytes 4259840 | tf_op jit(solution)/shard_map/all_to_all | solution.py:30
  17.1 9.8 %collective-permute-start.2 = (bf16[32,256]{1,0:T(8,128)(2,1)S(1)}, bf16[32,256]{1,0:T(8,128)(2,1)S(1)}, u32[]{:S(2)}, u32[]{:S(2)}) collective-permute-start(bf16[32,256]{1,0:T(8,128)(2,1)S(1)} %copy-done.6), channel_id=1, source_target_pairs={{0,384},{128,0},{256,128},{384,256},{1,385},{129,1},{257,129},{385... | collective-permute-start | bytes 49160 | tf_op jit(solution)/shard_map/ppermute | solution.py:35
  26.8 1.9 %collective-permute-start.1 = (bf16[32,256]{1,0:T(8,128)(2,1)S(1)}, bf16[32,256]{1,0:T(8,128)(2,1)S(1)}, u32[]{:S(2)}, u32[]{:S(2)}) collective-permute-start(bf16[32,256]{1,0:T(8,128)(2,1)S(1)} %copy-done.6), channel_id=1, source_target_pairs={{0,256},{128,384},{256,0},{384,128},{1,257},{129,385},{257,1},{385... | collective-permute-start | bytes 49160 | tf_op jit(solution)/shard_map/ppermute | solution.py:35
  28.8 4.2 %collective-permute-start = (bf16[32,256]{1,0:T(8,128)(2,1)S(1)}, bf16[32,256]{1,0:T(8,128)(2,1)S(1)}, u32[]{:S(2)}, u32[]{:S(2)}) collective-permute-start(bf16[32,256]{1,0:T(8,128)(2,1)S(1)} %copy-done.6), channel_id=1, source_target_pairs={{0,128},{128,256},{256,384},{384,0},{1,129},{129,257},{257,385},{3... | collective-permute-start | bytes 49160 | tf_op jit(solution)/shard_map/ppermute | solution.py:35
  33.1 0.6 stack.103.at_ref
  33.7 0.0 collective-permute-done.2
  33.7 16.2 %collective-permute-done.1 = bf16[32,256]{1,0:T(8,128)(2,1)S(1)} collective-permute-done((bf16[32,256]{1,0:T(8,128)(2,1)S(1)}, bf16[32,256]{1,0:T(8,128)(2,1)S(1)}, u32[]{:S(2)}, u32[]{:S(2)}) %collective-permute-start.1) | collective-permute-done | bytes 16416 | tf_op jit(solution)/shard_map/ppermute | solution.py:35
  49.9 0.0 collective-permute-done
  49.9 5.0 %collective-permute-start.5 = (bf16[4,32,256]{2,1,0:T(8,128)(2,1)S(1)}, bf16[4,32,256]{2,1,0:T(8,128)(2,1)S(1)}, u32[]{:S(2)}, u32[]{:S(2)}) collective-permute-start(bf16[4,32,256]{2,1,0:T(8,128)(2,1)S(1)} %get-tuple-element.47), channel_id=1, source_target_pairs={{0,48},{16,0},{32,16},{48,32},{1,49},{17,1},{33,17},{49,33},{2,50}... | collective-permute-start | bytes 196616 | tf_op jit(solution)/shard_map/ppermute | solution.py:35
  54.9 4.4 %collective-permute-start.4 = (bf16[4,32,256]{2,1,0:T(8,128)(2,1)S(1)}, bf16[4,32,256]{2,1,0:T(8,128)(2,1)S(1)}, u32[]{:S(2)}, u32[]{:S(2)}) collective-permute-start(bf16[4,32,256]{2,1,0:T(8,128)(2,1)S(1)} %get-tuple-element.47), channel_id=1, source_target_pairs={{0,32},{16,48},{32,0},{48,16},{1,33},{17,49},{33,1},{49,17},{2,34}... | collective-permute-start | bytes 196616 | tf_op jit(solution)/shard_map/ppermute | solution.py:35
  59.4 3.3 %collective-permute-start.3 = (bf16[4,32,256]{2,1,0:T(8,128)(2,1)S(1)}, bf16[4,32,256]{2,1,0:T(8,128)(2,1)S(1)}, u32[]{:S(2)}, u32[]{:S(2)}) collective-permute-start(bf16[4,32,256]{2,1,0:T(8,128)(2,1)S(1)} %get-tuple-element.47), channel_id=1, source_target_pairs={{0,16},{16,32},{32,48},{48,0},{1,17},{17,33},{33,49},{49,1},{2,18}... | collective-permute-start | bytes 196616 | tf_op jit(solution)/shard_map/ppermute | solution.py:35
  62.7 0.0 collective-permute-done.5
  62.7 1.1 collective-permute-done.4
  63.9 4.0 %collective-permute-done.3 = bf16[4,32,256]{2,1,0:T(8,128)(2,1)S(1)} collective-permute-done((bf16[4,32,256]{2,1,0:T(8,128)(2,1)S(1)}, bf16[4,32,256]{2,1,0:T(8,128)(2,1)S(1)}, u32[]{:S(2)}, u32[]{:S(2)}) %collective-permute-start.3) | collective-permute-done | bytes 65568 | tf_op jit(solution)/shard_map/ppermute | solution.py:35
  67.9 0.7 pad_maximum_fusion.p_ref
  68.6 1.4 copy-done
  70.0 3.5 %second.1 = bf16[16,72,128]{2,1,0:T(8,128)(2,1)} custom-call(s32[6]{0:T(128)} %stack.103.at_ref, bf16[4,4,32,256]{3,2,1,0:T(8,128)(2,1)} %pad_maximum_fusion.p_ref, bf16[16,520,128]{2,1,0:T(8,128)(2,1)} %copy-done), custom_call_target="tpu_custom_call" | custom-call | tf_op jit(solution)/shard_map/second/pallas_call | solution.py:263
  73.5 4.8 %all-to-all-start.1 = ((bf16[16,72,128]{2,1,0:T(8,128)(2,1)}), bf16[16,72,128]{2,1,0:T(8,128)(2,1)S(1)}, u32[]{:S(2)}, u32[]{:S(2)}) async-start(bf16[16,72,128]{2,1,0:T(8,128)(2,1)} %second.1), calls=%async_computation.1 | async-start | bytes 589824 | tf_op jit(solution)/shard_map/all_to_all | solution.py:30
  78.4 4.4 %collective-permute-start.8 = (f32[128,128]{1,0:T(8,128)S(1)}, f32[128,128]{1,0:T(8,128)S(1)}, u32[]{:S(2)}, u32[]{:S(2)}) collective-permute-start(f32[128,128]{1,0:T(8,128)S(1)} %get-tuple-element.43), channel_id=1, source_target_pairs={{0,6},{2,0},{4,2},{6,4},{1,7},{3,1},{5,3},{7,5},{8,14},{10,8},{12,... | collective-permute-start | bytes 196616 | tf_op jit(solution)/shard_map/ppermute | solution.py:35
  82.8 2.8 %collective-permute-start.7 = (f32[128,128]{1,0:T(8,128)S(1)}, f32[128,128]{1,0:T(8,128)S(1)}, u32[]{:S(2)}, u32[]{:S(2)}) collective-permute-start(f32[128,128]{1,0:T(8,128)S(1)} %get-tuple-element.44), channel_id=1, source_target_pairs={{0,4},{2,6},{4,0},{6,2},{1,5},{3,7},{5,1},{7,3},{8,12},{10,14},{12... | collective-permute-start | bytes 196616 | tf_op jit(solution)/shard_map/ppermute | solution.py:35
  85.6 2.3 %collective-permute-start.6 = (f32[128,128]{1,0:T(8,128)S(1)}, f32[128,128]{1,0:T(8,128)S(1)}, u32[]{:S(2)}, u32[]{:S(2)}) collective-permute-start(f32[128,128]{1,0:T(8,128)S(1)} %get-tuple-element.45), channel_id=1, source_target_pairs={{0,2},{2,4},{4,6},{6,0},{1,3},{3,5},{5,7},{7,1},{8,10},{10,12},{12... | collective-permute-start | bytes 196616 | tf_op jit(solution)/shard_map/ppermute | solution.py:35
  87.8 0.0 collective-permute-done.8
  87.9 1.7 %collective-permute-done.7 = f32[128,128]{1,0:T(8,128)S(1)} collective-permute-done((f32[128,128]{1,0:T(8,128)S(1)}, f32[128,128]{1,0:T(8,128)S(1)}, u32[]{:S(2)}, u32[]{:S(2)}) %collective-permute-start.7) | collective-permute-done | bytes 65568 | tf_op jit(solution)/shard_map/ppermute | solution.py:35
  89.6 2.5 %collective-permute-done.6 = f32[128,128]{1,0:T(8,128)S(1)} collective-permute-done((f32[128,128]{1,0:T(8,128)S(1)}, f32[128,128]{1,0:T(8,128)S(1)}, u32[]{:S(2)}, u32[]{:S(2)}) %collective-permute-start.6) | collective-permute-done | bytes 65568 | tf_op jit(solution)/shard_map/ppermute | solution.py:35
  92.1 0.7 pad_maximum_fusion.1.moments_ref
  92.8 0.0 all-to-all-done.1.in_ref
  92.8 0.7 copy-done.2
  93.5 1.7 %third.1 = (f32[32,128]{1,0:T(8,128)}, bf16[64,16,128]{2,1,0:T(8,128)(2,1)}, f32[8,128]{1,0:T(8,128)}) custom-call(bf16[16,72,128]{2,1,0:T(8,128)(2,1)} %copy-done.2), custom_call_target="tpu_custom_call" | custom-call | tf_op jit(solution)/shard_map/third/pallas_call | solution.py:280
  95.2 13.8 %all-to-all-start.2 = ((bf16[64,16,128]{2,1,0:T(8,128)(2,1)}), bf16[64,16,128]{2,1,0:T(8,128)(2,1)S(1)}, u32[]{:S(2)}, u32[]{:S(2)}) async-start(bf16[64,16,128]{2,1,0:T(8,128)(2,1)} %get-tuple-element.28), calls=%async_computation.2 | async-start | bytes 524288 | tf_op jit(solution)/shard_map/all_to_all | solution.py:30
  109.0 1.9 %collective-permute-start.11 = (f32[8,128]{1,0:T(8,128)}, f32[8,128]{1,0:T(8,128)S(1)}, u32[]{:S(2)}, u32[]{:S(2)}) collective-permute-start(f32[8,128]{1,0:T(8,128)} %get-tuple-element.29), channel_id=1, source_target_pairs={{0,6},{2,0},{4,2},{6,4},{1,7},{3,1},{5,3},{7,5},{8,14},{10,8},{12,... | collective-permute-start | bytes 12296 | tf_op jit(solution)/shard_map/ppermute | solution.py:35
  111.0 2.5 %collective-permute-start.10 = (f32[8,128]{1,0:T(8,128)}, f32[8,128]{1,0:T(8,128)S(1)}, u32[]{:S(2)}, u32[]{:S(2)}) collective-permute-start(f32[8,128]{1,0:T(8,128)} %get-tuple-element.29), channel_id=1, source_target_pairs={{0,4},{2,6},{4,0},{6,2},{1,5},{3,7},{5,1},{7,3},{8,12},{10,14},{12... | collective-permute-start | bytes 12296 | tf_op jit(solution)/shard_map/ppermute | solution.py:35
  113.5 2.8 %collective-permute-start.9 = (f32[8,128]{1,0:T(8,128)}, f32[8,128]{1,0:T(8,128)S(1)}, u32[]{:S(2)}, u32[]{:S(2)}) collective-permute-start(f32[8,128]{1,0:T(8,128)} %get-tuple-element.29), channel_id=1, source_target_pairs={{0,2},{2,4},{4,6},{6,0},{1,3},{3,5},{5,7},{7,1},{8,10},{10,12},{12... | collective-permute-start | bytes 12296 | tf_op jit(solution)/shard_map/ppermute | solution.py:35
  116.3 0.8 collective-permute-done.10
  117.0 3.1 %collective-permute-done.9 = f32[8,128]{1,0:T(8,128)S(1)} collective-permute-done((f32[8,128]{1,0:T(8,128)}, f32[8,128]{1,0:T(8,128)S(1)}, u32[]{:S(2)}, u32[]{:S(2)}) %collective-permute-start.9) | collective-permute-done | bytes 4128 | tf_op jit(solution)/shard_map/ppermute | solution.py:35
  120.1 0.7 fusion.1
  120.8 2.9 %collective-permute-start.12 = (f32[4,8,128]{2,1,0:T(8,128)S(1)}, f32[4,8,128]{2,1,0:T(8,128)S(1)}, u32[]{:S(2)}, u32[]{:S(2)}) collective-permute-start(f32[4,8,128]{2,1,0:T(8,128)S(1)} %get-tuple-element.51), channel_id=1, source_target_pairs={{0,8},{8,0},{1,9},{9,1},{2,10},{10,2},{3,11},{11,3},{4,12},{12,4},... | collective-permute-start | bytes 49160 | tf_op jit(solution)/shard_map/ppermute | solution.py:35
  123.7 1.9 %collective-permute-done.12 = f32[4,8,128]{2,1,0:T(8,128)S(1)} collective-permute-done((f32[4,8,128]{2,1,0:T(8,128)S(1)}, f32[4,8,128]{2,1,0:T(8,128)S(1)}, u32[]{:S(2)}, u32[]{:S(2)}) %collective-permute-start.12) | collective-permute-done | bytes 16416 | tf_op jit(solution)/shard_map/ppermute | solution.py:35
  125.6 2.9 %collective-permute-start.13 = (f32[2,4,8,128]{3,2,1,0:T(8,128)S(1)}, f32[2,4,8,128]{3,2,1,0:T(8,128)S(1)}, u32[]{:S(2)}, u32[]{:S(2)}) collective-permute-start(f32[2,4,8,128]{3,2,1,0:T(8,128)S(1)} %get-tuple-element.49), channel_id=1, source_target_pairs={{0,64},{64,0},{1,65},{65,1},{2,66},{66,2},{3,67},{67,3},{4,68},{68... | collective-permute-start | bytes 98312 | tf_op jit(solution)/shard_map/ppermute | solution.py:35
  128.5 1.7 %collective-permute-done.13 = f32[2,4,8,128]{3,2,1,0:T(8,128)S(1)} collective-permute-done((f32[2,4,8,128]{3,2,1,0:T(8,128)S(1)}, f32[2,4,8,128]{3,2,1,0:T(8,128)S(1)}, u32[]{:S(2)}, u32[]{:S(2)}) %collective-permute-start.13) | collective-permute-done | bytes 32800 | tf_op jit(solution)/shard_map/ppermute | solution.py:35
  130.2 0.6 pad_maximum_fusion.3.in_ref
  130.9 0.7 copy-done.3
  131.6 2.2 %fourth.1 = f32[8,136,128]{2,1,0:T(8,128)} custom-call(s32[6]{0:T(128)} %stack.103.at_ref, bf16[64,16,128]{2,1,0:T(8,128)(2,1)} %copy-done.3, f32[4,128,128]{2,1,0:T(8,128)} %pad_maximum_fusion.1.moments_ref, bf16[32,256]{1,0:T(8,128)(2,1)} %p_ref.1, f32[32,128]{1,0:T(8,128)} %get-tuple-element.32.gradient_ref), custom_call_target="tpu_custom_call" | custom-call | tf_op jit(solution)/shard_map/fourth/pallas_call | solution.py:295
  133.7 12.2 %all-to-all-start.3 = ((f32[8,136,128]{2,1,0:T(8,128)}), f32[8,136,128]{2,1,0:T(8,128)S(1)}, u32[]{:S(2)}, u32[]{:S(2)}) async-start(f32[8,136,128]{2,1,0:T(8,128)} %fourth.1), calls=%async_computation.3 | async-start | bytes 1114112 | tf_op jit(solution)/shard_map/all_to_all | solution.py:30
  146.0 1.7 %gating.1 = (f32[8,2048]{1,0:T(8,128)}, f32[8,2048]{1,0:T(8,128)}, f32[8,2048]{1,0:T(8,128)}) custom-call(s32[6]{0:T(128)} %stack.103.at_ref, f32[2,2,4,8,128]{4,3,2,1,0:T(8,128)} %pad_maximum_fusion.3.in_ref, f32[8,2048]{1,0:T(8,128)} %mean_ref.3, f32[8,2048]{1,0:T(8,128)} %square_ref.3), custom_call_target="tpu_custom_call" | custom-call | tf_op jit(solution)/shard_map/gating/pallas_call | solution.py:305
  147.6 8.1 %all-to-all-done.3.in_ref = f32[8,136,128]{2,1,0:T(8,128)S(1)} async-done(((f32[8,136,128]{2,1,0:T(8,128)}), f32[8,136,128]{2,1,0:T(8,128)S(1)}, u32[]{:S(2)}, u32[]{:S(2)}) %all-to-all-start.3) | async-done | bytes 557088 | tf_op jit(solution)/shard_map/all_to_all | solution.py:30
  155.7 0.8 copy-done.1
  156.5 2.0 %last.1 = (f32[32,512]{1,0:T(8,128)}, f32[32,512]{1,0:T(8,128)}, bf16[32,512]{1,0:T(8,128)(2,1)}, f32[64,512]{1,0:T(8,128)}, f32[64,512]{1,0:T(8,128)}) custom-call(s32[6]{0:T(128)} %stack.103.at_ref, f32[8,136,128]{2,1,0:T(8,128)} %copy-done.1, f32[32,512]{1,0:T(8,128)} %master_ref.1, f32[64,512]{1,0:T(8,128)} %mean_ref.2, f32[64,512]{1,0:T(8,128)} %square_ref.2), custom_call_target="tpu_custom_call" | custom-call | tf_op jit(solution)/shard_map/last/pallas_call | solution.py:313
  (18 shorter events, 0.1 us)
Async XLA Ops:
  9.1 7.9 %copy-start.6 = (bf16[32,256]{1,0:T(8,128)(2,1)S(1)}, bf16[32,256]{1,0:T(8,128)(2,1)}, u32[]{:S(2)}) copy-start(bf16[32,256]{1,0:T(8,128)(2,1)} %p_ref.1) | copy-start | bytes 49156
  9.1 23.9 %copy-start.4 = (f32[64,512]{1,0:T(8,128)S(1)}, f32[64,512]{1,0:T(8,128)}, u32[]{:S(2)}) copy-start(f32[64,512]{1,0:T(8,128)} %mean_ref.2) | copy-start | bytes 393220
  9.1 23.9 %copy-start.5 = (f32[64,512]{1,0:T(8,128)S(1)}, f32[64,512]{1,0:T(8,128)}, u32[]{:S(2)}) copy-start(f32[64,512]{1,0:T(8,128)} %square_ref.2) | copy-start | bytes 393220
  9.1 59.5 %all-to-all-start = ((bf16[16,520,128]{2,1,0:T(8,128)(2,1)}), bf16[16,520,128]{2,1,0:T(8,128)(2,1)S(1)}, u32[]{:S(2)}, u32[]{:S(2)}) async-start(bf16[16,520,128]{2,1,0:T(8,128)(2,1)} %first.1), calls=%async_computation | async-start | bytes 4259840 | tf_op jit(solution)/shard_map/all_to_all | solution.py:30
  17.1 16.6 %collective-permute-start.2 = (bf16[32,256]{1,0:T(8,128)(2,1)S(1)}, bf16[32,256]{1,0:T(8,128)(2,1)S(1)}, u32[]{:S(2)}, u32[]{:S(2)}) collective-permute-start(bf16[32,256]{1,0:T(8,128)(2,1)S(1)} %copy-done.6), channel_id=1, source_target_pairs={{0,384},{128,0},{256,128},{384,256},{1,385},{129,1},{257,129},{385... | collective-permute-start | bytes 49160 | tf_op jit(solution)/shard_map/ppermute | solution.py:35
  26.8 23.1 %collective-permute-start.1 = (bf16[32,256]{1,0:T(8,128)(2,1)S(1)}, bf16[32,256]{1,0:T(8,128)(2,1)S(1)}, u32[]{:S(2)}, u32[]{:S(2)}) collective-permute-start(bf16[32,256]{1,0:T(8,128)(2,1)S(1)} %copy-done.6), channel_id=1, source_target_pairs={{0,256},{128,384},{256,0},{384,128},{1,257},{129,385},{257,1},{385... | collective-permute-start | bytes 49160 | tf_op jit(solution)/shard_map/ppermute | solution.py:35
  28.8 21.2 %collective-permute-start = (bf16[32,256]{1,0:T(8,128)(2,1)S(1)}, bf16[32,256]{1,0:T(8,128)(2,1)S(1)}, u32[]{:S(2)}, u32[]{:S(2)}) collective-permute-start(bf16[32,256]{1,0:T(8,128)(2,1)S(1)} %copy-done.6), channel_id=1, source_target_pairs={{0,128},{128,256},{256,384},{384,0},{1,129},{129,257},{257,385},{3... | collective-permute-start | bytes 49160 | tf_op jit(solution)/shard_map/ppermute | solution.py:35
  49.9 12.8 %collective-permute-start.5 = (bf16[4,32,256]{2,1,0:T(8,128)(2,1)S(1)}, bf16[4,32,256]{2,1,0:T(8,128)(2,1)S(1)}, u32[]{:S(2)}, u32[]{:S(2)}) collective-permute-start(bf16[4,32,256]{2,1,0:T(8,128)(2,1)S(1)} %get-tuple-element.47), channel_id=1, source_target_pairs={{0,48},{16,0},{32,16},{48,32},{1,49},{17,1},{33,17},{49,33},{2,50}... | collective-permute-start | bytes 196616 | tf_op jit(solution)/shard_map/ppermute | solution.py:35
  54.9 8.9 %collective-permute-start.4 = (bf16[4,32,256]{2,1,0:T(8,128)(2,1)S(1)}, bf16[4,32,256]{2,1,0:T(8,128)(2,1)S(1)}, u32[]{:S(2)}, u32[]{:S(2)}) collective-permute-start(bf16[4,32,256]{2,1,0:T(8,128)(2,1)S(1)} %get-tuple-element.47), channel_id=1, source_target_pairs={{0,32},{16,48},{32,0},{48,16},{1,33},{17,49},{33,1},{49,17},{2,34}... | collective-permute-start | bytes 196616 | tf_op jit(solution)/shard_map/ppermute | solution.py:35
  59.4 8.5 %collective-permute-start.3 = (bf16[4,32,256]{2,1,0:T(8,128)(2,1)S(1)}, bf16[4,32,256]{2,1,0:T(8,128)(2,1)S(1)}, u32[]{:S(2)}, u32[]{:S(2)}) collective-permute-start(bf16[4,32,256]{2,1,0:T(8,128)(2,1)S(1)} %get-tuple-element.47), channel_id=1, source_target_pairs={{0,16},{16,32},{32,48},{48,0},{1,17},{17,33},{33,49},{49,1},{2,18}... | collective-permute-start | bytes 196616 | tf_op jit(solution)/shard_map/ppermute | solution.py:35
  68.6 1.4 copy-start
  73.5 19.3 %all-to-all-start.1 = ((bf16[16,72,128]{2,1,0:T(8,128)(2,1)}), bf16[16,72,128]{2,1,0:T(8,128)(2,1)S(1)}, u32[]{:S(2)}, u32[]{:S(2)}) async-start(bf16[16,72,128]{2,1,0:T(8,128)(2,1)} %second.1), calls=%async_computation.1 | async-start | bytes 589824 | tf_op jit(solution)/shard_map/all_to_all | solution.py:30
  78.4 9.5 %collective-permute-start.8 = (f32[128,128]{1,0:T(8,128)S(1)}, f32[128,128]{1,0:T(8,128)S(1)}, u32[]{:S(2)}, u32[]{:S(2)}) collective-permute-start(f32[128,128]{1,0:T(8,128)S(1)} %get-tuple-element.43), channel_id=1, source_target_pairs={{0,6},{2,0},{4,2},{6,4},{1,7},{3,1},{5,3},{7,5},{8,14},{10,8},{12,... | collective-permute-start | bytes 196616 | tf_op jit(solution)/shard_map/ppermute | solution.py:35
  82.8 6.8 %collective-permute-start.7 = (f32[128,128]{1,0:T(8,128)S(1)}, f32[128,128]{1,0:T(8,128)S(1)}, u32[]{:S(2)}, u32[]{:S(2)}) collective-permute-start(f32[128,128]{1,0:T(8,128)S(1)} %get-tuple-element.44), channel_id=1, source_target_pairs={{0,4},{2,6},{4,0},{6,2},{1,5},{3,7},{5,1},{7,3},{8,12},{10,14},{12... | collective-permute-start | bytes 196616 | tf_op jit(solution)/shard_map/ppermute | solution.py:35
  85.6 6.5 %collective-permute-start.6 = (f32[128,128]{1,0:T(8,128)S(1)}, f32[128,128]{1,0:T(8,128)S(1)}, u32[]{:S(2)}, u32[]{:S(2)}) collective-permute-start(f32[128,128]{1,0:T(8,128)S(1)} %get-tuple-element.45), channel_id=1, source_target_pairs={{0,2},{2,4},{4,6},{6,0},{1,3},{3,5},{5,7},{7,1},{8,10},{10,12},{12... | collective-permute-start | bytes 196616 | tf_op jit(solution)/shard_map/ppermute | solution.py:35
  92.8 0.7 copy-start.2
  95.2 35.6 %all-to-all-start.2 = ((bf16[64,16,128]{2,1,0:T(8,128)(2,1)}), bf16[64,16,128]{2,1,0:T(8,128)(2,1)S(1)}, u32[]{:S(2)}, u32[]{:S(2)}) async-start(bf16[64,16,128]{2,1,0:T(8,128)(2,1)} %get-tuple-element.28), calls=%async_computation.2 | async-start | bytes 524288 | tf_op jit(solution)/shard_map/all_to_all | solution.py:30
  109.0 7.2 %collective-permute-start.11 = (f32[8,128]{1,0:T(8,128)}, f32[8,128]{1,0:T(8,128)S(1)}, u32[]{:S(2)}, u32[]{:S(2)}) collective-permute-start(f32[8,128]{1,0:T(8,128)} %get-tuple-element.29), channel_id=1, source_target_pairs={{0,6},{2,0},{4,2},{6,4},{1,7},{3,1},{5,3},{7,5},{8,14},{10,8},{12,... | collective-permute-start | bytes 12296 | tf_op jit(solution)/shard_map/ppermute | solution.py:35
  111.0 6.1 %collective-permute-start.10 = (f32[8,128]{1,0:T(8,128)}, f32[8,128]{1,0:T(8,128)S(1)}, u32[]{:S(2)}, u32[]{:S(2)}) collective-permute-start(f32[8,128]{1,0:T(8,128)} %get-tuple-element.29), channel_id=1, source_target_pairs={{0,4},{2,6},{4,0},{6,2},{1,5},{3,7},{5,1},{7,3},{8,12},{10,14},{12... | collective-permute-start | bytes 12296 | tf_op jit(solution)/shard_map/ppermute | solution.py:35
  113.5 6.7 %collective-permute-start.9 = (f32[8,128]{1,0:T(8,128)}, f32[8,128]{1,0:T(8,128)S(1)}, u32[]{:S(2)}, u32[]{:S(2)}) collective-permute-start(f32[8,128]{1,0:T(8,128)} %get-tuple-element.29), channel_id=1, source_target_pairs={{0,2},{2,4},{4,6},{6,0},{1,3},{3,5},{5,7},{7,1},{8,10},{10,12},{12... | collective-permute-start | bytes 12296 | tf_op jit(solution)/shard_map/ppermute | solution.py:35
  120.8 4.8 %collective-permute-start.12 = (f32[4,8,128]{2,1,0:T(8,128)S(1)}, f32[4,8,128]{2,1,0:T(8,128)S(1)}, u32[]{:S(2)}, u32[]{:S(2)}) collective-permute-start(f32[4,8,128]{2,1,0:T(8,128)S(1)} %get-tuple-element.51), channel_id=1, source_target_pairs={{0,8},{8,0},{1,9},{9,1},{2,10},{10,2},{3,11},{11,3},{4,12},{12,4},... | collective-permute-start | bytes 49160 | tf_op jit(solution)/shard_map/ppermute | solution.py:35
  125.6 4.6 %collective-permute-start.13 = (f32[2,4,8,128]{3,2,1,0:T(8,128)S(1)}, f32[2,4,8,128]{3,2,1,0:T(8,128)S(1)}, u32[]{:S(2)}, u32[]{:S(2)}) collective-permute-start(f32[2,4,8,128]{3,2,1,0:T(8,128)S(1)} %get-tuple-element.49), channel_id=1, source_target_pairs={{0,64},{64,0},{1,65},{65,1},{2,66},{66,2},{3,67},{67,3},{4,68},{68... | collective-permute-start | bytes 98312 | tf_op jit(solution)/shard_map/ppermute | solution.py:35
  130.9 0.7 copy-start.3
  133.7 22.0 %all-to-all-start.3 = ((f32[8,136,128]{2,1,0:T(8,128)}), f32[8,136,128]{2,1,0:T(8,128)S(1)}, u32[]{:S(2)}, u32[]{:S(2)}) async-start(f32[8,136,128]{2,1,0:T(8,128)} %fourth.1), calls=%async_computation.3 | async-start | bytes 1114112 | tf_op jit(solution)/shard_map/all_to_all | solution.py:30
  155.7 0.8 copy-start.1

commit v3 on v2

v3 whole, which is shorter than its diff:
```python
import functools

import jax
import jax.numpy as jnp
from jax import lax
from jax.experimental import pallas as pl
from jax.experimental.pallas import tpu as pltpu
from jax.sharding import Mesh
from jax.sharding import PartitionSpec as P

FS = ("zh", "zl", "yh", "yl")
NEAR = ("zl", "yl", "x")
FAR = ("zh", "yh")
PAIR = ("x", "c")

BETA_ONE = 0.9
BETA_TWO = 0.95
STEP_RATE = 0.01
EPSILON = 1e-08
NORM_FLOOR = 1e-06
BF = jnp.bfloat16
F32 = jnp.float32
FIRST = (((0,), (0,)), ((), ()))
LANES = 128
VMEM = pl.BlockSpec(memory_space=pltpu.VMEM)
ANY = pl.BlockSpec(memory_space=pltpu.HBM)
SMEM = pl.BlockSpec(memory_space=pltpu.SMEM)


def swap(pieces, axes):
    return lax.all_to_all(pieces, axes, 0, 0, tiled=True)


def shifted(value, axis, step):
    length = lax.axis_size(axis)
    return lax.ppermute(value, axis, [(i, (i + step) % length) for i in range(length)])


def turned(value, axis):
    steps = range(1, lax.axis_size(axis))
    return jnp.stack([value, *(shifted(value, axis, s) for s in steps)])


def split_two(v):
    high = v.astype(BF)
    return high, (v - high.astype(F32)).astype(BF)


def dot(a, b, dims=(((1,), (0,)), ((), ()))):
    return lax.dot_general(a, b, dims, preferred_element_type=F32)


def one_less_exp(v):
    series = 1.0 + v * 0.125
    for k in range(7, 1, -1):
        series = 1.0 + v * (1.0 / k) * series
    return jnp.where(v > -0.3, -v * series, 1.0 - jnp.exp(v))


def gate_signals(cot, totals):
    heads, tokens = cot.shape
    later = lax.broadcasted_iota(jnp.int32, (tokens, tokens), 0) >= lax.broadcasted_iota(
        jnp.int32, (tokens, tokens), 1
    )
    later = jnp.where(later, 1.0, 0.0).astype(BF)
    one = cot.astype(BF).astype(F32)
    rest = cot - one
    two = rest.astype(BF).astype(F32)
    parts = jnp.concatenate([one, two, rest - two, jnp.zeros_like(one)], axis=0).astype(BF)
    trailing = dot(parts, later)
    trailing = trailing[2 * heads : 3 * heads] + trailing[heads : 2 * heads] + trailing[:heads]
    lane = lax.broadcasted_iota(jnp.int32, totals.shape, 1)
    gate = totals - jnp.where(lane == 0, 0.0, pltpu.roll(totals, 1, 1))
    return (trailing * one_less_exp(gate)).astype(BF)


def first_kernel(
    sizes, x_ref, q_ref, cot_ref, tot_ref, out_ref, x_held, q_held, out_held, gate_held, x_sem, q_sem, out_sem
):
    nz, nzl, ny, nyl, nx, own = sizes
    wide = x_held.shape[2]
    heads, steps = gate_held.shape[1], nz * nzl
    copies = []
    q_copy = pltpu.make_async_copy(q_ref, q_held, q_sem)
    q_copy.start()
    for z in range(steps):
        copy = pltpu.make_async_copy(x_ref.at[:, z * wide : (z + 1) * wide], x_held.at[z], x_sem.at[z])
        copy.start()
        copies.append(copy)
    signal = gate_signals(cot_ref[...], tot_ref[...])
    q_copy.wait()
    sends = []
    for z in range(steps):
        copies[z].wait()
        block = x_held[z]
        part = dot(block, q_held[...], FIRST).astype(BF)
        zh, zl = divmod(z, nzl)
        for yh in range(ny):
            for yl in range(nyl):
                row = (yh * nyl + yl) * own
                for q in range(nx):
                    out_held[z, yl * nx + q, yh * own : (yh + 1) * own, :] = part[
                        row : row + own, q * LANES : (q + 1) * LANES
                    ]
        target = out_ref.at[
            zl * nyl * nx : (zl + 1) * nyl * nx, zh * ny * own : (zh + 1) * ny * own, :
        ]
        send = pltpu.make_async_copy(out_held.at[z], target, out_sem.at[z])
        send.start()
        sends.append(send)
        gates = dot(signal, block).astype(BF)
        for k in range(wide // LANES):
            gate_held[z * (wide // LANES) + k] = gates[:, k * LANES : (k + 1) * LANES]
    target = out_ref.at[:, nz * ny * own : nz * ny * own + heads, :]
    send = pltpu.make_async_copy(gate_held, target, out_sem.at[steps])
    send.start()
    sends.append(send)
    for send in sends:
        send.wait()


def second_kernel(own, in_ref, out_ref):
    far, rows = out_ref.shape[:2]
    for k in range(far + 1):
        cut = slice(k * own, (k + 1) * own) if k < far else slice(far * own, in_ref.shape[1])
        summed = in_ref[0, cut].astype(F32)
        for i in range(1, in_ref.shape[0]):
            summed = summed + in_ref[i, cut].astype(F32)
        if k < far:
            out_ref[k, :own, :] = summed.astype(BF)
        else:
            for j in range(far):
                out_ref[j, own:, :] = summed.astype(BF)


def third_kernel(norming, in_ref, p_ref, gradient_ref, out_ref, gate_ref):
    own = p_ref.shape[0]
    summed = in_ref[0].astype(F32)
    for k in range(1, in_ref.shape[0]):
        summed = summed + in_ref[k].astype(F32)
    summed = summed * norming
    gate_ref[...] = summed[own:]
    gradient = summed[:own]
    gradient_ref[...] = gradient
    factor = p_ref[...]
    high, low = split_two(gradient)
    rank = dot(factor, high, FIRST) + dot(factor, low, FIRST)
    top = lax.broadcasted_iota(jnp.int32, (8, LANES), 0) < 4
    for g in range(out_ref.shape[0] // 2):
        value = rank[8 * g : 8 * g + 8]
        high = value.astype(BF).astype(F32)
        low = value - high
        out_ref[2 * g] = jnp.where(top, high, pltpu.roll(low, 4, 0)).astype(BF)
        out_ref[2 * g + 1] = jnp.where(top, pltpu.roll(high, 4, 0), low).astype(BF)


def rank_kernel(in_ref, out_ref):
    summed = in_ref[0].astype(F32)
    for k in range(1, in_ref.shape[0]):
        summed = summed + in_ref[k].astype(F32)
    summed = summed + pltpu.roll(summed, 4, 0)
    high = summed.astype(BF).astype(F32)
    top = lax.broadcasted_iota(jnp.int32, (8, LANES), 0) < 4
    piece = jnp.where(top, high, summed - high).astype(BF)
    for k in range(out_ref.shape[0]):
        out_ref[k] = piece


def fourth_kernel(
    sizes, at_ref, in_ref, moments_ref, p_ref, gradient_ref, gates_ref, out_ref, projected, direction
):
    nx, nc = sizes
    top = lax.broadcasted_iota(jnp.int32, (8, LANES), 0) < 4
    for g in range(in_ref.shape[0] // 2):
        even, odd = in_ref[2 * g].astype(F32), in_ref[2 * g + 1].astype(F32)
        even = even + pltpu.roll(even, 4, 0)
        odd = odd + pltpu.roll(odd, 4, 0)
        projected[8 * g : 8 * g + 8, :] = jnp.where(top, even, odd)
    block = projected.shape[0] // nx
    squares = jnp.zeros((2, LANES), F32)
    for s in range(nx):
        where = pl.multiple_of(lax.rem(at_ref[0] + nx - s, nx) * block, block)
        p = projected[pl.ds(where, block), :]
        mean = BETA_ONE * moments_ref[s, :block] + (1.0 - BETA_ONE) * p
        square = BETA_TWO * moments_ref[s, block:] + (1.0 - BETA_TWO) * p * p
        d = mean / (jnp.sqrt(square) + EPSILON)
        direction[pl.ds(where, block), :] = d
        squares = squares + jnp.concatenate(
            [jnp.sum(d * d, axis=0, keepdims=True), jnp.sum(p * p, axis=0, keepdims=True)], axis=0
        )
    factor = p_ref[...]
    own = factor.shape[0]
    high, low = split_two(direction[...])
    lifted_direction = dot(factor, high) + dot(factor, low)
    high, low = split_two(projected[...])
    lifted_projected = dot(factor, high) + dot(factor, low) - gradient_ref[...]
    squares = jnp.concatenate([squares, jnp.zeros((6, LANES), F32)], axis=0)
    gates = gates_ref[...].reshape(-1, LANES)
    for x in range(nx):
        for c in range(nc):
            k = x * nc + c
            out_ref[k, :own] = lifted_direction
            out_ref[k, own : 2 * own] = lifted_projected
            out_ref[k, 2 * own : 2 * own + block] = projected[x * block : (x + 1) * block, :]
            out_ref[k, 2 * own + block : 2 * own + block + 8] = squares
            out_ref[k, 2 * own + block + 8 :] = gates


def last_kernel(
    sizes,
    at_ref,
    in_ref,
    master_ref,
    mean_ref,
    square_ref,
    gate_mean_ref,
    gate_square_ref,
    update_ref,
    new_ref,
    copy_ref,
    mean_out,
    square_out,
    gate_update_ref,
    average_ref,
    energy_ref,
):
    nzl, nyl, nx, nc, own, block = sizes
    heads = gate_mean_ref.shape[0]
    after = 2 * own + block + 8
    squares = in_ref[0, 2 * own + block : after]
    for k in range(1, nx * nc):
        squares = squares + in_ref[k, 2 * own + block : after]
    direction_squares = jnp.sum(squares[0:1], axis=1, keepdims=True)
    projected_squares = jnp.sum(squares[1:2], axis=1, keepdims=True)
    balance = jnp.sqrt(direction_squares / (projected_squares + NORM_FLOOR))
    for x in range(nx):
        k = x * nc + at_ref[1]
        cut = slice(x * LANES, (x + 1) * LANES)
        update = in_ref[k, :own] - balance * in_ref[k, own : 2 * own]
        update_ref[:, cut] = update
        new = master_ref[:, cut] - STEP_RATE * update
        new_ref[:, cut] = new
        copy_ref[:, cut] = new.astype(BF)
        p = in_ref[k, 2 * own : 2 * own + block]
        mean_out[:, cut] = BETA_ONE * mean_ref[:, cut] + (1.0 - BETA_ONE) * p
        square_out[:, cut] = BETA_TWO * square_ref[:, cut] + (1.0 - BETA_TWO) * p * p
        for a in range(nzl):
            for b in range(nyl):
                zl = lax.rem(at_ref[2] + nzl - a, nzl)
                yl = lax.rem(at_ref[3] + nyl - b, nyl)
                place = pl.ds(pl.multiple_of(((zl * nyl + yl) * nx + x) * LANES, LANES), LANES)
                row = after + (a * nyl + b) * heads
                g = in_ref[k, row : row + heads]
                average = BETA_ONE * gate_mean_ref[:, place] + (1.0 - BETA_ONE) * g
                energy = BETA_TWO * gate_square_ref[:, place] + (1.0 - BETA_TWO) * g * g
                average_ref[:, place] = average
                energy_ref[:, place] = energy
                gate_update_ref[:, place] = average / (jnp.sqrt(energy) + EPSILON)


def near_memory(value):
    return pltpu.with_memory_space_constraint(value, pltpu.VMEM)


def per_device(
    attention_input,
    query_cotangent,
    gate_cotangent,
    gate_totals,
    projector,
    query_master,
    lowrank_mean,
    lowrank_square,
    gating_mean,
    gating_square,
):
    nz, ny, nzl, nyl, nx, nc = (lax.axis_size(a) for a in ("zh", "yh", "zl", "yl", "x", "c"))
    far, near = nz * ny, nzl * nyl * nx
    every = far * nzl * nyl
    tokens, width = attention_input.shape
    columns = query_cotangent.shape[1]
    heads = gate_cotangent.shape[0]
    own, rank = projector.shape
    block = rank // nx
    norming = 1.0 / (tokens * far * near) ** 0.5
    shape = jax.ShapeDtypeStruct
    at = jnp.stack([lax.axis_index(a) for a in ("x", "c", "zl", "yl")]).astype(jnp.int32)

    wide = ny * nyl * own
    first = pl.pallas_call(
        functools.partial(first_kernel, (nz, nzl, ny, nyl, nx, own)),
        out_shape=shape((near, far * own + heads, LANES), BF),
        in_specs=[ANY, ANY, VMEM, VMEM],
        out_specs=ANY,
        scratch_shapes=[
            pltpu.VMEM((nz * nzl, tokens, wide), BF),
            pltpu.VMEM((tokens, columns), BF),
            pltpu.VMEM((nz * nzl, nyl * nx, ny * own, LANES), BF),
            pltpu.VMEM((near, heads, LANES), BF),
            pltpu.SemaphoreType.DMA((nz * nzl,)),
            pltpu.SemaphoreType.DMA,
            pltpu.SemaphoreType.DMA((nz * nzl + 1,)),
        ],
        name="first",
    )(attention_input, query_cotangent, gate_cotangent, gate_totals)
    first = swap(first, NEAR)

    second = pl.pallas_call(
        functools.partial(second_kernel, own),
        out_shape=pltpu.VMEM((far, own + heads, LANES), BF),
        in_specs=[VMEM],
        out_specs=VMEM,
        name="second",
    )(near_memory(first))
    mine = jnp.concatenate(
        [lowrank_mean.reshape(block, nx, LANES), lowrank_square.reshape(block, nx, LANES)]
    ).transpose(1, 0, 2)
    place = lax.axis_index("x")
    pieces = [lax.dynamic_index_in_dim(mine, lax.rem(place + s, nx), 0, False) for s in range(nx)]
    first, pieces = lax.optimization_barrier((first, pieces))
    second = swap(second, FAR)
    moments = jnp.stack([pieces[0], *(shifted(pieces[s], "x", s) for s in range(1, nx))])
    second, moments = lax.optimization_barrier((second, moments))

    gradient, third, gates = pl.pallas_call(
        functools.partial(third_kernel, norming),
        out_shape=(
            pltpu.VMEM((own, LANES), F32),
            pltpu.VMEM((every, 8, LANES), BF),
            pltpu.VMEM((heads, LANES), F32),
        ),
        in_specs=[VMEM, VMEM],
        out_specs=(VMEM, VMEM, VMEM),
        name="third",
    )(near_memory(second), projector)
    third = swap(third, FS)
    gates = turned(gates, "yl")
    third, gates = lax.optimization_barrier((third, gates))

    ranked = pl.pallas_call(
        rank_kernel,
        out_shape=pltpu.VMEM((every, 8, LANES), BF),
        in_specs=[VMEM],
        out_specs=VMEM,
        name="ranked",
    )(near_memory(third))
    ranked = swap(ranked, FS)
    gates = turned(gates, "zl")
    ranked, gates = lax.optimization_barrier((ranked, gates))

    fourth = pl.pallas_call(
        functools.partial(fourth_kernel, (nx, nc)),
        out_shape=pltpu.VMEM((nx * nc, 2 * own + block + 8 + nzl * nyl * heads, LANES), F32),
        in_specs=[SMEM, VMEM, VMEM, VMEM, VMEM, VMEM],
        out_specs=VMEM,
        scratch_shapes=[pltpu.VMEM((rank, LANES), F32), pltpu.VMEM((rank, LANES), F32)],
        name="fourth",
    )(at, near_memory(ranked), near_memory(moments), projector, gradient, near_memory(gates))
    fourth = swap(fourth, PAIR)

    return pl.pallas_call(
        functools.partial(last_kernel, (nzl, nyl, nx, nc, own, block)),
        out_shape=(
            shape((own, columns), F32),
            shape((own, columns), F32),
            shape((own, columns), BF),
            shape((block, columns), F32),
            shape((block, columns), F32),
            shape((heads, width), F32),
            shape((heads, width), F32),
            shape((heads, width), F32),
        ),
        in_specs=[SMEM, *[VMEM] * 6],
        out_specs=(VMEM,) * 8,
        name="last",
    )(at, near_memory(fourth), query_master, lowrank_mean, lowrank_square, gating_mean, gating_square)


def solution(mesh):
    split = Mesh(
        mesh.devices.reshape(4, 2, 4, 2, mesh.shape["rep"], mesh.shape["tp"]),
        ("zh", "zl", "yh", "yl", "x", "c"),
    )
    in_specs = (
        P((*FS, "x"), None),
        P((*FS, "x"), "c"),
        P("c", (*FS, "x")),
        P("c", (*FS, "x")),
        P(FS, None),
        P(FS, "c"),
        P("x", "c"),
        P("x", "c"),
        P("c", None),
        P("c", None),
    )
    out_specs = (
        P(FS, "c"),
        P(FS, "c"),
        P(FS, "c"),
        P("x", "c"),
        P("x", "c"),
        P("c", None),
        P("c", None),
        P("c", None),
    )
    return jax.shard_map(
        per_device, mesh=split, in_specs=in_specs, out_specs=out_specs, check_vma=False
    )
```

time: 160 us -> 138 us (0.86)
  starting transfers between devices: 89.8 us -> 53.3 us
  blocking collectives: 0 us -> 20.8 us
  waiting for transfers between devices: 41.1 us -> 48.2 us
  Pallas kernels: 19.5 us -> 13.4 us
  local copies, waits for them, and re-layouts: 4.29 us -> 0.67 us
  other arithmetic: 2.84 us -> 0.59 us
    ppermute x14 -> x5, starting transfers between devices: 51.1 us -> 14.1 us  [shifted(): lax.ppermute(value, axis, [(i, (i + step) % length) for i in range(length)])]
    all_to_all x4, waiting for transfers between devices: 8.08 us -> 41.6 us  [swap(): return lax.all_to_all(pieces, axes, 0, 0, tiled=True)]
    ppermute x14 -> x5, waiting for transfers between devices: 33.1 us -> 6.64 us  [shifted(): lax.ppermute(value, axis, [(i, (i + step) % length) for i in range(length)])]
    all_to_all x0 -> x1, blocking collectives: none -> 20.8 us  [swap(): return lax.all_to_all(pieces, axes, 0, 0, tiled=True)]
    pallas_call x6, Pallas kernels: 19.5 us -> 13.4 us  [the longest x1 7.09 us: per_device(): pl.pallas_call(functools.partial(first_kernel, (nz, nzl, ny, nyl, nx, own...]
    unnamed x14 -> x7, local copies, waits for them, and re-layouts: 3.62 us -> 0.63 us
    another operation x5 -> x2, other arithmetic: 2.09 us -> 0.01 us  [turned(): return jnp.stack([value, *(shifted(value, axis, s) for s in steps)])]
  transfers between devices with their start and end apart: 18 -> 9, of which waited for: 10 -> 7; matrix products, arithmetic and copies ran while one was open for 2% -> 0% of each run, Pallas kernels for 1% -> 0%
where the time goes in v3:
time: 138 us
  starting transfers between devices  53.3 us (39%)
  waiting for transfers between devices  48.2 us (35%)
  blocking collectives  20.8 us (15%)
  Pallas kernels  13.4 us (10%)
    all_to_all x4, waiting for transfers between devices, swap(): return lax.all_to_all(pieces, axes, 0, 0, tiled=True)  41.6 us
    all_to_all x4, starting transfers between devices, swap(): return lax.all_to_all(pieces, axes, 0, 0, tiled=True)  39.2 us
    all_to_all x1, blocking collectives, swap(): return lax.all_to_all(pieces, axes, 0, 0, tiled=True)  20.8 us
    ppermute x5, starting transfers between devices, shifted(): lax.ppermute(value, axis, [(i, (i + step) % length) for i in range(length)])  14.1 us
    pallas_call x1, Pallas kernels, per_device(): pl.pallas_call(functools.partial(first_kernel, (nz, nzl, ny, nyl, nx, own...  7.09 us
    ppermute x5, waiting for transfers between devices, shifted(): lax.ppermute(value, axis, [(i, (i + step) % length) for i in range(length)])  6.64 us
  transfers between devices with their start and end apart: 9, of which 7 were waited for; matrix products, arithmetic and copies ran while one was open for 0% of the time, Pallas kernels for 0%

profile of v3, /device:TPU:1, one launch (start us, length us, event | category | flops | bytes accessed | tf_op | source)
XLA Modules:
  0.0 137.8 jit_solution(15938073657979884979)
XLA Ops:
  0.6 7.1 %first.1 = bf16[16,520,128]{2,1,0:T(8,128)(2,1)} custom-call(bf16[768,2048]{1,0:T(8,128)(2,1)} %x_ref.1, bf16[768,512]{1,0:T(8,128)(2,1)} %q_ref.1, f32[8,768]{1,0:T(8,128)} %cot_ref.1, f32[8,768]{1,0:T(8,128)} %tot_ref.1), custom_call_target="tpu_custom_call" | custom-call | tf_op jit(solution)/shard_map/first/pallas_call | solution.py:290
  7.7 0.0 copy-start.1
  7.7 7.9 %all-to-all-start = ((bf16[16,520,128]{2,1,0:T(8,128)(2,1)}), bf16[16,520,128]{2,1,0:T(8,128)(2,1)S(1)}, u32[]{:S(2)}, u32[]{:S(2)}) async-start(bf16[16,520,128]{2,1,0:T(8,128)(2,1)} %first.1), calls=%async_computation | async-start | bytes 4259840 | tf_op jit(solution)/shard_map/all_to_all | solution.py:31
  15.7 0.0 copy-done.1
  15.7 0.0 copy-start.2
  15.7 27.3 %all-to-all-done.in_ref = bf16[16,520,128]{2,1,0:T(8,128)(2,1)S(1)} async-done(((bf16[16,520,128]{2,1,0:T(8,128)(2,1)}), bf16[16,520,128]{2,1,0:T(8,128)(2,1)S(1)}, u32[]{:S(2)}, u32[]{:S(2)}) %all-to-all-start) | async-done | bytes 2129952 | tf_op jit(solution)/shard_map/all_to_all | solution.py:31
  43.0 1.0 second.1
  43.9 14.2 %all-to-all-start.1 = ((bf16[16,40,128]{2,1,0:T(8,128)(2,1)}), bf16[16,40,128]{2,1,0:T(8,128)(2,1)S(1)}, u32[]{:S(2)}, u32[]{:S(2)}) async-start(bf16[16,40,128]{2,1,0:T(8,128)(2,1)} %second.1), calls=%async_computation.1 | async-start | bytes 327680 | tf_op jit(solution)/shard_map/all_to_all | solution.py:31
  58.1 0.0 copy-done.2
  58.2 3.3 %collective-permute-start.2 = (f32[128,128]{1,0:T(8,128)S(1)}, f32[128,128]{1,0:T(8,128)S(1)}, u32[]{:S(2)}, u32[]{:S(2)}) collective-permute-start(f32[128,128]{1,0:T(8,128)S(1)} %get-tuple-element.24), channel_id=1, source_target_pairs={{0,6},{2,0},{4,2},{6,4},{1,7},{3,1},{5,3},{7,5},{8,14},{10,8},{12,... | collective-permute-start | bytes 196616 | tf_op jit(solution)/shard_map/ppermute | solution.py:36
  61.5 2.5 %collective-permute-start.1 = (f32[128,128]{1,0:T(8,128)S(1)}, f32[128,128]{1,0:T(8,128)S(1)}, u32[]{:S(2)}, u32[]{:S(2)}) collective-permute-start(f32[128,128]{1,0:T(8,128)S(1)} %get-tuple-element.23), channel_id=1, source_target_pairs={{0,4},{2,6},{4,0},{6,2},{1,5},{3,7},{5,1},{7,3},{8,12},{10,14},{12... | collective-permute-start | bytes 196616 | tf_op jit(solution)/shard_map/ppermute | solution.py:36
  64.1 2.4 %collective-permute-start = (f32[128,128]{1,0:T(8,128)S(1)}, f32[128,128]{1,0:T(8,128)S(1)}, u32[]{:S(2)}, u32[]{:S(2)}) collective-permute-start(f32[128,128]{1,0:T(8,128)S(1)} %get-tuple-element.22), channel_id=1, source_target_pairs={{0,2},{2,4},{4,6},{6,0},{1,3},{3,5},{5,7},{7,1},{8,10},{10,12},{12... | collective-permute-start | bytes 196616 | tf_op jit(solution)/shard_map/ppermute | solution.py:36
  66.5 0.0 collective-permute-done.2
  66.5 1.9 %collective-permute-done.1 = f32[128,128]{1,0:T(8,128)S(1)} collective-permute-done((f32[128,128]{1,0:T(8,128)S(1)}, f32[128,128]{1,0:T(8,128)S(1)}, u32[]{:S(2)}, u32[]{:S(2)}) %collective-permute-start.1) | collective-permute-done | bytes 65568 | tf_op jit(solution)/shard_map/ppermute | solution.py:36
  68.3 2.5 %collective-permute-done = f32[128,128]{1,0:T(8,128)S(1)} collective-permute-done((f32[128,128]{1,0:T(8,128)S(1)}, f32[128,128]{1,0:T(8,128)S(1)}, u32[]{:S(2)}, u32[]{:S(2)}) %collective-permute-start) | collective-permute-done | bytes 65568 | tf_op jit(solution)/shard_map/ppermute | solution.py:36
  70.8 0.0 all-to-all-done.1.in_ref
  70.8 1.6 %third.1 = (f32[32,128]{1,0:T(8,128)S(1)}, bf16[64,8,128]{2,1,0:T(8,128)(2,1)}, f32[8,128]{1,0:T(8,128)S(1)}) custom-call(bf16[16,40,128]{2,1,0:T(8,128)(2,1)S(1)} %all-to-all-done.1.in_ref, bf16[32,256]{1,0:T(8,128)(2,1)} %p_ref.3), custom_call_target="tpu_custom_call" | custom-call | tf_op jit(solution)/shard_map/third/pallas_call | solution.py:325
  72.4 0.0 copy-start
  72.4 0.6 copy-done
  73.0 11.9 %all-to-all-start.2 = ((bf16[64,8,128]{2,1,0:T(8,128)(2,1)}), bf16[64,8,128]{2,1,0:T(8,128)(2,1)S(1)}, u32[]{:S(2)}, u32[]{:S(2)}) async-start(bf16[64,8,128]{2,1,0:T(8,128)(2,1)} %get-tuple-element.26), calls=%async_computation.2 | async-start | bytes 262144 | tf_op jit(solution)/shard_map/all_to_all | solution.py:31
  84.9 2.9 %collective-permute-start.3 = (f32[8,128]{1,0:T(8,128)S(1)}, f32[8,128]{1,0:T(8,128)S(1)}, u32[]{:S(2)}, u32[]{:S(2)}) collective-permute-start(f32[8,128]{1,0:T(8,128)S(1)} %get-tuple-element.27), channel_id=1, source_target_pairs={{0,8},{8,0},{1,9},{9,1},{2,10},{10,2},{3,11},{11,3},{4,12},{12,4},... | collective-permute-start | bytes 12296 | tf_op jit(solution)/shard_map/ppermute | solution.py:36
  87.8 1.4 %collective-permute-done.3 = f32[8,128]{1,0:T(8,128)S(1)} collective-permute-done((f32[8,128]{1,0:T(8,128)S(1)}, f32[8,128]{1,0:T(8,128)S(1)}, u32[]{:S(2)}, u32[]{:S(2)}) %collective-permute-start.3) | collective-permute-done | bytes 4128 | tf_op jit(solution)/shard_map/ppermute | solution.py:36
  89.2 7.2 %all-to-all-done.2.in_ref = bf16[64,8,128]{2,1,0:T(8,128)(2,1)S(1)} async-done(((bf16[64,8,128]{2,1,0:T(8,128)(2,1)}), bf16[64,8,128]{2,1,0:T(8,128)(2,1)S(1)}, u32[]{:S(2)}, u32[]{:S(2)}) %all-to-all-start.2) | async-done | bytes 131104 | tf_op jit(solution)/shard_map/all_to_all | solution.py:31
  96.4 0.7 ranked.1
  97.2 5.3 %all-to-all-start.3 = ((bf16[64,8,128]{2,1,0:T(8,128)(2,1)}), bf16[64,8,128]{2,1,0:T(8,128)(2,1)S(1)}, u32[]{:S(2)}, u32[]{:S(2)}) async-start(bf16[64,8,128]{2,1,0:T(8,128)(2,1)} %ranked.1), calls=%async_computation.3 | async-start | bytes 262144 | tf_op jit(solution)/shard_map/all_to_all | solution.py:31
  102.4 2.9 %collective-permute-start.4 = (f32[2,8,128]{2,1,0:T(8,128)S(1)}, f32[2,8,128]{2,1,0:T(8,128)S(1)}, u32[]{:S(2)}, u32[]{:S(2)}) collective-permute-start(f32[2,8,128]{2,1,0:T(8,128)S(1)} %pad_maximum_fusion.2), channel_id=1, source_target_pairs={{0,64},{64,0},{1,65},{65,1},{2,66},{66,2},{3,67},{67,3},{4,68},{68... | collective-permute-start | bytes 24584 | tf_op jit(solution)/shard_map/ppermute | solution.py:36
  105.4 0.6 pad_add_fusion.at_ref
  105.9 0.9 collective-permute-done.4
  106.8 7.1 %all-to-all-done.3.in_ref = bf16[64,8,128]{2,1,0:T(8,128)(2,1)S(1)} async-done(((bf16[64,8,128]{2,1,0:T(8,128)(2,1)}), bf16[64,8,128]{2,1,0:T(8,128)(2,1)S(1)}, u32[]{:S(2)}, u32[]{:S(2)}) %all-to-all-start.3) | async-done | bytes 131104 | tf_op jit(solution)/shard_map/all_to_all | solution.py:31
  114.0 1.1 fourth.1
  115.0 20.8 %all_to_all.25.in_ref = f32[8,168,128]{2,1,0:T(8,128)S(1)} all-to-all(f32[8,168,128]{2,1,0:T(8,128)S(1)} %fourth.1), channel_id=1, replica_groups=mesh['zh'=4,'zl'=2,'yh'=4,'yl'=2,'x'=4,'c'=2] {'x','c'}, dimensions={0} | all-to-all | bytes 1376256 | tf_op jit(solution)/shard_map/all_to_all | solution.py:31
  135.8 2.0 %last.1 = (f32[32,512]{1,0:T(8,128)}, f32[32,512]{1,0:T(8,128)}, bf16[32,512]{1,0:T(8,128)(2,1)}, f32[64,512]{1,0:T(8,128)}, f32[64,512]{1,0:T(8,128)}, /*index=...) custom-call(s32[4]{0:T(128)} %pad_add_fusion.at_ref, f32[8,168,128]{2,1,0:T(8,128)S(1)} %all_to_all.25.in_ref, ...), custom_call_target="tpu_custom_call" | custom-call | tf_op jit(solution)/shard_map/last/pallas_call | solution.py:361
  (6 shorter events, 0.1 us)
Async XLA Ops:
  7.7 7.9 %copy-start.1 = (f32[64,512]{1,0:T(8,128)S(1)}, f32[64,512]{1,0:T(8,128)}, u32[]{:S(2)}) copy-start(f32[64,512]{1,0:T(8,128)} %mean_ref.1) | copy-start | bytes 393220
  7.7 35.2 %all-to-all-start = ((bf16[16,520,128]{2,1,0:T(8,128)(2,1)}), bf16[16,520,128]{2,1,0:T(8,128)(2,1)S(1)}, u32[]{:S(2)}, u32[]{:S(2)}) async-start(bf16[16,520,128]{2,1,0:T(8,128)(2,1)} %first.1), calls=%async_computation | async-start | bytes 4259840 | tf_op jit(solution)/shard_map/all_to_all | solution.py:31
  15.7 42.5 %copy-start.2 = (f32[64,512]{1,0:T(8,128)S(1)}, f32[64,512]{1,0:T(8,128)}, u32[]{:S(2)}) copy-start(f32[64,512]{1,0:T(8,128)} %square_ref.1) | copy-start | bytes 393220
  43.9 26.9 %all-to-all-start.1 = ((bf16[16,40,128]{2,1,0:T(8,128)(2,1)}), bf16[16,40,128]{2,1,0:T(8,128)(2,1)S(1)}, u32[]{:S(2)}, u32[]{:S(2)}) async-start(bf16[16,40,128]{2,1,0:T(8,128)(2,1)} %second.1), calls=%async_computation.1 | async-start | bytes 327680 | tf_op jit(solution)/shard_map/all_to_all | solution.py:31
  58.2 8.3 %collective-permute-start.2 = (f32[128,128]{1,0:T(8,128)S(1)}, f32[128,128]{1,0:T(8,128)S(1)}, u32[]{:S(2)}, u32[]{:S(2)}) collective-permute-start(f32[128,128]{1,0:T(8,128)S(1)} %get-tuple-element.24), channel_id=1, source_target_pairs={{0,6},{2,0},{4,2},{6,4},{1,7},{3,1},{5,3},{7,5},{8,14},{10,8},{12,... | collective-permute-start | bytes 196616 | tf_op jit(solution)/shard_map/ppermute | solution.py:36
  61.5 6.8 %collective-permute-start.1 = (f32[128,128]{1,0:T(8,128)S(1)}, f32[128,128]{1,0:T(8,128)S(1)}, u32[]{:S(2)}, u32[]{:S(2)}) collective-permute-start(f32[128,128]{1,0:T(8,128)S(1)} %get-tuple-element.23), channel_id=1, source_target_pairs={{0,4},{2,6},{4,0},{6,2},{1,5},{3,7},{5,1},{7,3},{8,12},{10,14},{12... | collective-permute-start | bytes 196616 | tf_op jit(solution)/shard_map/ppermute | solution.py:36
  64.1 6.7 %collective-permute-start = (f32[128,128]{1,0:T(8,128)S(1)}, f32[128,128]{1,0:T(8,128)S(1)}, u32[]{:S(2)}, u32[]{:S(2)}) collective-permute-start(f32[128,128]{1,0:T(8,128)S(1)} %get-tuple-element.22), channel_id=1, source_target_pairs={{0,2},{2,4},{4,6},{6,0},{1,3},{3,5},{5,7},{7,1},{8,10},{10,12},{12... | collective-permute-start | bytes 196616 | tf_op jit(solution)/shard_map/ppermute | solution.py:36
  72.4 0.6 copy-start
  73.0 23.4 %all-to-all-start.2 = ((bf16[64,8,128]{2,1,0:T(8,128)(2,1)}), bf16[64,8,128]{2,1,0:T(8,128)(2,1)S(1)}, u32[]{:S(2)}, u32[]{:S(2)}) async-start(bf16[64,8,128]{2,1,0:T(8,128)(2,1)} %get-tuple-element.26), calls=%async_computation.2 | async-start | bytes 262144 | tf_op jit(solution)/shard_map/all_to_all | solution.py:31
  84.9 4.4 %collective-permute-start.3 = (f32[8,128]{1,0:T(8,128)S(1)}, f32[8,128]{1,0:T(8,128)S(1)}, u32[]{:S(2)}, u32[]{:S(2)}) collective-permute-start(f32[8,128]{1,0:T(8,128)S(1)} %get-tuple-element.27), channel_id=1, source_target_pairs={{0,8},{8,0},{1,9},{9,1},{2,10},{10,2},{3,11},{11,3},{4,12},{12,4},... | collective-permute-start | bytes 12296 | tf_op jit(solution)/shard_map/ppermute | solution.py:36
  97.2 16.8 %all-to-all-start.3 = ((bf16[64,8,128]{2,1,0:T(8,128)(2,1)}), bf16[64,8,128]{2,1,0:T(8,128)(2,1)S(1)}, u32[]{:S(2)}, u32[]{:S(2)}) async-start(bf16[64,8,128]{2,1,0:T(8,128)(2,1)} %ranked.1), calls=%async_computation.3 | async-start | bytes 262144 | tf_op jit(solution)/shard_map/all_to_all | solution.py:31
  102.4 4.4 %collective-permute-start.4 = (f32[2,8,128]{2,1,0:T(8,128)S(1)}, f32[2,8,128]{2,1,0:T(8,128)S(1)}, u32[]{:S(2)}, u32[]{:S(2)}) collective-permute-start(f32[2,8,128]{2,1,0:T(8,128)S(1)} %pad_maximum_fusion.2), channel_id=1, source_target_pairs={{0,64},{64,0},{1,65},{65,1},{2,66},{66,2},{3,67},{67,3},{4,68},{68... | collective-permute-start | bytes 24584 | tf_op jit(solution)/shard_map/ppermute | solution.py:36

commit v4 on v3

--- a/solution.py
+++ b/solution.py
@@ -34,11 +34,6 @@
 def shifted(value, axis, step):
     length = lax.axis_size(axis)
     return lax.ppermute(value, axis, [(i, (i + step) % length) for i in range(length)])
-
-
-def turned(value, axis):
-    steps = range(1, lax.axis_size(axis))
-    return jnp.stack([value, *(shifted(value, axis, s) for s in steps)])
 
 
 def split_two(v):
@@ -154,28 +149,40 @@
         out_ref[2 * g + 1] = jnp.where(top, pltpu.roll(high, 4, 0), low).astype(BF)
 
 
-def rank_kernel(in_ref, out_ref):
+def rank_kernel(at_ref, in_ref, gates_ref, out_ref, held):
     summed = in_ref[0].astype(F32)
     for k in range(1, in_ref.shape[0]):
         summed = summed + in_ref[k].astype(F32)
     summed = summed + pltpu.roll(summed, 4, 0)
-    high = summed.astype(BF).astype(F32)
+    gates = gates_ref[...]
+    high = gates.astype(BF).astype(F32)
+    low = gates - high
+    held[0] = pltpu.roll(high, 4, 0)
+    held[1] = high
+    held[2] = pltpu.roll(low, 4, 0)
+    held[3] = low
     top = lax.broadcasted_iota(jnp.int32, (8, LANES), 0) < 4
-    piece = jnp.where(top, high, summed - high).astype(BF)
+    piece = jnp.where(top, summed, held[lax.rem(at_ref[4], 4)]).astype(BF)
     for k in range(out_ref.shape[0]):
         out_ref[k] = piece
 
 
 def fourth_kernel(
-    sizes, at_ref, in_ref, moments_ref, p_ref, gradient_ref, gates_ref, out_ref, projected, direction
+    sizes, at_ref, in_ref, moments_ref, p_ref, gradient_ref, out_ref, projected, direction, gates
 ):
-    nx, nc = sizes
+    nzl, ny, nyl, nx, nc = sizes
     top = lax.broadcasted_iota(jnp.int32, (8, LANES), 0) < 4
     for g in range(in_ref.shape[0] // 2):
         even, odd = in_ref[2 * g].astype(F32), in_ref[2 * g + 1].astype(F32)
-        even = even + pltpu.roll(even, 4, 0)
-        odd = odd + pltpu.roll(odd, 4, 0)
-        projected[8 * g : 8 * g + 8, :] = jnp.where(top, even, odd)
+        projected[8 * g : 8 * g + 8, :] = jnp.where(top, even, pltpu.roll(odd, 4, 0))
+    for zl in range(nzl):
+        for yl in range(nyl):
+            one, two, three, four = (
+                in_ref[(zl * ny + yh) * nyl + yl].astype(F32) for yh in range(4)
+            )
+            gates[8 * (zl * nyl + yl) : 8 * (zl * nyl + yl) + 8, :] = jnp.where(
+                top, pltpu.roll(one, 4, 0) + pltpu.roll(three, 4, 0), two + four
+            )
     block = projected.shape[0] // nx
     squares = jnp.zeros((2, LANES), F32)
     for s in range(nx):
@@ -195,7 +202,6 @@
     high, low = split_two(projected[...])
     lifted_projected = dot(factor, high) + dot(factor, low) - gradient_ref[...]
     squares = jnp.concatenate([squares, jnp.zeros((6, LANES), F32)], axis=0)
-    gates = gates_ref[...].reshape(-1, LANES)
     for x in range(nx):
         for c in range(nc):
             k = x * nc + c
@@ -203,7 +209,7 @@
             out_ref[k, own : 2 * own] = lifted_projected
             out_ref[k, 2 * own : 2 * own + block] = projected[x * block : (x + 1) * block, :]
             out_ref[k, 2 * own + block : 2 * own + block + 8] = squares
-            out_ref[k, 2 * own + block + 8 :] = gates
+            out_ref[k, 2 * own + block + 8 :] = gates[...]
 
 
 def last_kernel(
@@ -246,9 +252,8 @@
         square_out[:, cut] = BETA_TWO * square_ref[:, cut] + (1.0 - BETA_TWO) * p * p
         for a in range(nzl):
             for b in range(nyl):
-                zl = lax.rem(at_ref[2] + nzl - a, nzl)
-                yl = lax.rem(at_ref[3] + nyl - b, nyl)
-                place = pl.ds(pl.multiple_of(((zl * nyl + yl) * nx + x) * LANES, LANES), LANES)
+                start = ((a * nyl + b) * nx + x) * LANES
+                place = slice(start, start + LANES)
                 row = after + (a * nyl + b) * heads
                 g = in_ref[k, row : row + heads]
                 average = BETA_ONE * gate_mean_ref[:, place] + (1.0 - BETA_ONE) * g
@@ -284,7 +289,7 @@
     block = rank // nx
     norming = 1.0 / (tokens * far * near) ** 0.5
     shape = jax.ShapeDtypeStruct
-    at = jnp.stack([lax.axis_index(a) for a in ("x", "c", "zl", "yl")]).astype(jnp.int32)
+    at = jnp.stack([lax.axis_index(a) for a in ("x", "c", "zl", "yl", "yh")]).astype(jnp.int32)
 
     wide = ny * nyl * own
     first = pl.pallas_call(
@@ -304,6 +309,13 @@
         name="first",
     )(attention_input, query_cotangent, gate_cotangent, gate_totals)
     first = swap(first, NEAR)
+    mine = jnp.concatenate(
+        [lowrank_mean.reshape(block, nx, LANES), lowrank_square.reshape(block, nx, LANES)]
+    ).transpose(1, 0, 2)
+    place = lax.axis_index("x")
+    pieces = [lax.dynamic_index_in_dim(mine, lax.rem(place + s, nx), 0, False) for s in range(nx)]
+    moments = jnp.stack([pieces[0], *(shifted(pieces[s], "x", s) for s in range(1, nx))])
+    first, moments = lax.optimization_barrier((first, moments))
 
     second = pl.pallas_call(
         functools.partial(second_kernel, own),
@@ -312,15 +324,7 @@
         out_specs=VMEM,
         name="second",
     )(near_memory(first))
-    mine = jnp.concatenate(
-        [lowrank_mean.reshape(block, nx, LANES), lowrank_square.reshape(block, nx, LANES)]
-    ).transpose(1, 0, 2)
-    place = lax.axis_index("x")
-    pieces = [lax.dynamic_index_in_dim(mine, lax.rem(place + s, nx), 0, False) for s in range(nx)]
-    first, pieces = lax.optimization_barrier((first, pieces))
     second = swap(second, FAR)
-    moments = jnp.stack([pieces[0], *(shifted(pieces[s], "x", s) for s in range(1, nx))])
-    second, moments = lax.optimization_barrier((second, moments))
 
     gradient, third, gates = pl.pallas_call(
         functools.partial(third_kernel, norming),
@@ -334,28 +338,29 @@
         name="third",
     )(near_memory(second), projector)
     third = swap(third, FS)
-    gates = turned(gates, "yl")
-    third, gates = lax.optimization_barrier((third, gates))
 
     ranked = pl.pallas_call(
         rank_kernel,
         out_shape=pltpu.VMEM((every, 8, LANES), BF),
-        in_specs=[VMEM],
+        in_specs=[SMEM, VMEM, VMEM],
         out_specs=VMEM,
+        scratch_shapes=[pltpu.VMEM((4, heads, LANES), F32)],
         name="ranked",
-    )(near_memory(third))
+    )(at, near_memory(third), near_memory(gates))
     ranked = swap(ranked, FS)
-    gates = turned(gates, "zl")
-    ranked, gates = lax.optimization_barrier((ranked, gates))
 
     fourth = pl.pallas_call(
-        functools.partial(fourth_kernel, (nx, nc)),
+        functools.partial(fourth_kernel, (nzl, ny, nyl, nx, nc)),
         out_shape=pltpu.VMEM((nx * nc, 2 * own + block + 8 + nzl * nyl * heads, LANES), F32),
-        in_specs=[SMEM, VMEM, VMEM, VMEM, VMEM, VMEM],
+        in_specs=[SMEM, VMEM, VMEM, VMEM, VMEM],
         out_specs=VMEM,
-        scratch_shapes=[pltpu.VMEM((rank, LANES), F32), pltpu.VMEM((rank, LANES), F32)],
+        scratch_shapes=[
+            pltpu.VMEM((rank, LANES), F32),
+            pltpu.VMEM((rank, LANES), F32),
+            pltpu.VMEM((nzl * nyl * heads, LANES), F32),
+        ],
         name="fourth",
-    )(at, near_memory(ranked), near_memory(moments), projector, gradient, near_memory(gates))
+    )(at, near_memory(ranked), near_memory(moments), projector, near_memory(gradient))
     fourth = swap(fourth, PAIR)
 
     return pl.pallas_call(

time: 138 us -> 128 us (0.928)
  blocking collectives: 20.8 us -> 59.1 us
  starting transfers between devices: 53.3 us -> 24.6 us
  waiting for transfers between devices: 48.2 us -> 29.2 us
    all_to_all x1 -> x3, blocking collectives: 20.8 us -> 59.1 us  [swap(): return lax.all_to_all(pieces, axes, 0, 0, tiled=True)]
    all_to_all x4 -> x2, waiting for transfers between devices: 41.6 us -> 10.9 us  [swap(): return lax.all_to_all(pieces, axes, 0, 0, tiled=True)]
    all_to_all x4 -> x2, starting transfers between devices: 39.2 us -> 15.2 us  [swap(): return lax.all_to_all(pieces, axes, 0, 0, tiled=True)]
    ppermute x5 -> x3, waiting for transfers between devices: 6.64 us -> 18.3 us  [shifted(): lax.ppermute(value, axis, [(i, (i + step) % length) for i in range(length)])]
    ppermute x5 -> x3, starting transfers between devices: 14.1 us -> 9.42 us  [shifted(): lax.ppermute(value, axis, [(i, (i + step) % length) for i in range(length)])]
  transfers between devices with their start and end apart: 9 -> 5, of which waited for: 7 -> 3; matrix products, arithmetic and copies ran while one was open for 0% -> 1% of each run, Pallas kernels for 0% -> 0%
where the time goes in v4:
time: 128 us; the launch traced here: 127 us
  blocking collectives  59.1 us (46%)
  waiting for transfers between devices  29.2 us (23%)
  starting transfers between devices  24.6 us (19%)
  Pallas kernels  12.7 us (10%)
    all_to_all x3, blocking collectives, swap(): return lax.all_to_all(pieces, axes, 0, 0, tiled=True)  59.1 us
    ppermute x3, waiting for transfers between devices, shifted(): lax.ppermute(value, axis, [(i, (i + step) % length) for i in range(length)])  18.3 us
    all_to_all x2, starting transfers between devices, swap(): return lax.all_to_all(pieces, axes, 0, 0, tiled=True)  15.2 us
    all_to_all x2, waiting for transfers between devices, swap(): return lax.all_to_all(pieces, axes, 0, 0, tiled=True)  10.9 us
    ppermute x3, starting transfers between devices, shifted(): lax.ppermute(value, axis, [(i, (i + step) % length) for i in range(length)])  9.42 us
    pallas_call x1, Pallas kernels, per_device(): pl.pallas_call(functools.partial(first_kernel, (nz, nzl, ny, nyl, nx, own...  7.08 us
  transfers between devices with their start and end apart: 5, of which 3 were waited for; matrix products, arithmetic and copies ran while one was open for 1% of the time, Pallas kernels for 0%

profile of v4, /device:TPU:1, one launch (start us, length us, event | category | flops | bytes accessed | tf_op | source)
XLA Modules:
  0.0 127.1 jit_solution(8404520238725276848)
XLA Ops:
  0.6 7.1 %first.1 = bf16[16,520,128]{2,1,0:T(8,128)(2,1)} custom-call(bf16[768,2048]{1,0:T(8,128)(2,1)} %x_ref.1, bf16[768,512]{1,0:T(8,128)(2,1)} %q_ref.1, f32[8,768]{1,0:T(8,128)} %cot_ref.1, f32[8,768]{1,0:T(8,128)} %tot_ref.1), custom_call_target="tpu_custom_call" | custom-call | tf_op jit(solution)/shard_map/first/pallas_call | solution.py:295
  7.7 0.0 copy-start
  7.7 0.0 copy-start.1
  7.7 7.9 %all-to-all-start = ((bf16[16,520,128]{2,1,0:T(8,128)(2,1)}), bf16[16,520,128]{2,1,0:T(8,128)(2,1)S(1)}, u32[]{:S(2)}, u32[]{:S(2)}) async-start(bf16[16,520,128]{2,1,0:T(8,128)(2,1)} %first.1), calls=%async_computation | async-start | bytes 4259840 | tf_op jit(solution)/shard_map/all_to_all | solution.py:31
  15.7 0.0 copy-done
  15.7 0.0 copy-done.1
  15.8 4.5 %collective-permute-start.2 = (f32[128,128]{1,0:T(8,128)S(1)}, f32[128,128]{1,0:T(8,128)S(1)}, u32[]{:S(2)}, u32[]{:S(2)}) collective-permute-start(f32[128,128]{1,0:T(8,128)S(1)} %get-tuple-element.19), channel_id=1, source_target_pairs={{0,6},{2,0},{4,2},{6,4},{1,7},{3,1},{5,3},{7,5},{8,14},{10,8},{12,... | collective-permute-start | bytes 196616 | tf_op jit(solution)/shard_map/ppermute | solution.py:36
  20.2 2.5 %collective-permute-start.1 = (f32[128,128]{1,0:T(8,128)S(1)}, f32[128,128]{1,0:T(8,128)S(1)}, u32[]{:S(2)}, u32[]{:S(2)}) collective-permute-start(f32[128,128]{1,0:T(8,128)S(1)} %get-tuple-element.20), channel_id=1, source_target_pairs={{0,4},{2,6},{4,0},{6,2},{1,5},{3,7},{5,1},{7,3},{8,12},{10,14},{12... | collective-permute-start | bytes 196616 | tf_op jit(solution)/shard_map/ppermute | solution.py:36
  22.7 2.5 %collective-permute-start = (f32[128,128]{1,0:T(8,128)S(1)}, f32[128,128]{1,0:T(8,128)S(1)}, u32[]{:S(2)}, u32[]{:S(2)}) collective-permute-start(f32[128,128]{1,0:T(8,128)S(1)} %get-tuple-element.21), channel_id=1, source_target_pairs={{0,2},{2,4},{4,6},{6,0},{1,3},{3,5},{5,7},{7,1},{8,10},{10,12},{12... | collective-permute-start | bytes 196616 | tf_op jit(solution)/shard_map/ppermute | solution.py:36
  25.2 0.0 collective-permute-done.2
  25.2 14.8 %collective-permute-done.1 = f32[128,128]{1,0:T(8,128)S(1)} collective-permute-done((f32[128,128]{1,0:T(8,128)S(1)}, f32[128,128]{1,0:T(8,128)S(1)}, u32[]{:S(2)}, u32[]{:S(2)}) %collective-permute-start.1) | collective-permute-done | bytes 65568 | tf_op jit(solution)/shard_map/ppermute | solution.py:36
  40.0 3.5 %collective-permute-done = f32[128,128]{1,0:T(8,128)S(1)} collective-permute-done((f32[128,128]{1,0:T(8,128)S(1)}, f32[128,128]{1,0:T(8,128)S(1)}, u32[]{:S(2)}, u32[]{:S(2)}) %collective-permute-start) | collective-permute-done | bytes 65568 | tf_op jit(solution)/shard_map/ppermute | solution.py:36
  43.5 0.0 all-to-all-done.in_ref
  43.5 0.3 second.1
  43.8 25.0 %all_to_all.25.in_ref = bf16[16,40,128]{2,1,0:T(8,128)(2,1)S(1)} all-to-all(bf16[16,40,128]{2,1,0:T(8,128)(2,1)S(1)} %second.1), channel_id=1, replica_groups=mesh['zh'=4,'zl'=2,'yh'=4,'yl'=2,'x'=4,'c'=2] {'zh','yh'}, dimensions={0} | all-to-all | bytes 327680 | tf_op jit(solution)/shard_map/all_to_all | solution.py:31
  68.8 1.6 %third.1 = (f32[32,128]{1,0:T(8,128)S(1)}, bf16[64,8,128]{2,1,0:T(8,128)(2,1)}, f32[8,128]{1,0:T(8,128)S(1)}) custom-call(bf16[16,40,128]{2,1,0:T(8,128)(2,1)S(1)} %all_to_all.25.in_ref, bf16[32,256]{1,0:T(8,128)(2,1)} %p_ref.3), custom_call_target="tpu_custom_call" | custom-call | tf_op jit(solution)/shard_map/third/pallas_call | solution.py:329
  70.4 7.3 %all-to-all-start.2 = ((bf16[64,8,128]{2,1,0:T(8,128)(2,1)}), bf16[64,8,128]{2,1,0:T(8,128)(2,1)S(1)}, u32[]{:S(2)}, u32[]{:S(2)}) async-start(bf16[64,8,128]{2,1,0:T(8,128)(2,1)} %get-tuple-element.14), calls=%async_computation.2 | async-start | bytes 262144 | tf_op jit(solution)/shard_map/all_to_all | solution.py:31
  77.7 0.6 stack.36.at_ref
  78.3 10.9 %all-to-all-done.2.in_ref = bf16[64,8,128]{2,1,0:T(8,128)(2,1)S(1)} async-done(((bf16[64,8,128]{2,1,0:T(8,128)(2,1)}), bf16[64,8,128]{2,1,0:T(8,128)(2,1)S(1)}, u32[]{:S(2)}, u32[]{:S(2)}) %all-to-all-start.2) | async-done | bytes 131104 | tf_op jit(solution)/shard_map/all_to_all | solution.py:31
  89.2 0.7 ranked.1
  90.0 15.3 %all_to_all.26.in_ref = bf16[64,8,128]{2,1,0:T(8,128)(2,1)S(1)} all-to-all(bf16[64,8,128]{2,1,0:T(8,128)(2,1)S(1)} %ranked.1), channel_id=1, replica_groups=mesh['zh'=4,'zl'=2,'yh'=4,'yl'=2,'x'=4,'c'=2] {'zh','zl','yh','yl'}, dimensions={0} | all-to-all | bytes 262144 | tf_op jit(solution)/shard_map/all_to_all | solution.py:31
  105.3 1.0 fourth.1
  106.3 18.8 %all_to_all.27.in_ref = f32[8,168,128]{2,1,0:T(8,128)S(1)} all-to-all(f32[8,168,128]{2,1,0:T(8,128)S(1)} %fourth.1), channel_id=1, replica_groups=mesh['zh'=4,'zl'=2,'yh'=4,'yl'=2,'x'=4,'c'=2] {'x','c'}, dimensions={0} | all-to-all | bytes 1376256 | tf_op jit(solution)/shard_map/all_to_all | solution.py:31
  125.1 1.9 %last.1 = (f32[32,512]{1,0:T(8,128)}, f32[32,512]{1,0:T(8,128)}, bf16[32,512]{1,0:T(8,128)(2,1)}, f32[64,512]{1,0:T(8,128)}, f32[64,512]{1,0:T(8,128)}, /*index=...) custom-call(s32[5]{0:T(128)} %stack.36.at_ref, f32[8,168,128]{2,1,0:T(8,128)S(1)} %all_to_all.27.in_ref, ...), custom_call_target="tpu_custom_call" | custom-call | tf_op jit(solution)/shard_map/last/pallas_call | solution.py:366
  (4 shorter events, 0.1 us)
Async XLA Ops:
  7.7 8.0 %copy-start = (f32[64,512]{1,0:T(8,128)S(1)}, f32[64,512]{1,0:T(8,128)}, u32[]{:S(2)}) copy-start(f32[64,512]{1,0:T(8,128)} %mean_ref.1) | copy-start | bytes 393220
  7.7 8.0 %copy-start.1 = (f32[64,512]{1,0:T(8,128)S(1)}, f32[64,512]{1,0:T(8,128)}, u32[]{:S(2)}) copy-start(f32[64,512]{1,0:T(8,128)} %square_ref.1) | copy-start | bytes 393220
  7.7 35.8 %all-to-all-start = ((bf16[16,520,128]{2,1,0:T(8,128)(2,1)}), bf16[16,520,128]{2,1,0:T(8,128)(2,1)S(1)}, u32[]{:S(2)}, u32[]{:S(2)}) async-start(bf16[16,520,128]{2,1,0:T(8,128)(2,1)} %first.1), calls=%async_computation | async-start | bytes 4259840 | tf_op jit(solution)/shard_map/all_to_all | solution.py:31
  15.8 9.4 %collective-permute-start.2 = (f32[128,128]{1,0:T(8,128)S(1)}, f32[128,128]{1,0:T(8,128)S(1)}, u32[]{:S(2)}, u32[]{:S(2)}) collective-permute-start(f32[128,128]{1,0:T(8,128)S(1)} %get-tuple-element.19), channel_id=1, source_target_pairs={{0,6},{2,0},{4,2},{6,4},{1,7},{3,1},{5,3},{7,5},{8,14},{10,8},{12,... | collective-permute-start | bytes 196616 | tf_op jit(solution)/shard_map/ppermute | solution.py:36
  20.2 19.8 %collective-permute-start.1 = (f32[128,128]{1,0:T(8,128)S(1)}, f32[128,128]{1,0:T(8,128)S(1)}, u32[]{:S(2)}, u32[]{:S(2)}) collective-permute-start(f32[128,128]{1,0:T(8,128)S(1)} %get-tuple-element.20), channel_id=1, source_target_pairs={{0,4},{2,6},{4,0},{6,2},{1,5},{3,7},{5,1},{7,3},{8,12},{10,14},{12... | collective-permute-start | bytes 196616 | tf_op jit(solution)/shard_map/ppermute | solution.py:36
  22.7 20.8 %collective-permute-start = (f32[128,128]{1,0:T(8,128)S(1)}, f32[128,128]{1,0:T(8,128)S(1)}, u32[]{:S(2)}, u32[]{:S(2)}) collective-permute-start(f32[128,128]{1,0:T(8,128)S(1)} %get-tuple-element.21), channel_id=1, source_target_pairs={{0,2},{2,4},{4,6},{6,0},{1,3},{3,5},{5,7},{7,1},{8,10},{10,12},{12... | collective-permute-start | bytes 196616 | tf_op jit(solution)/shard_map/ppermute | solution.py:36
  70.4 18.8 %all-to-all-start.2 = ((bf16[64,8,128]{2,1,0:T(8,128)(2,1)}), bf16[64,8,128]{2,1,0:T(8,128)(2,1)S(1)}, u32[]{:S(2)}, u32[]{:S(2)}) async-start(bf16[64,8,128]{2,1,0:T(8,128)(2,1)} %get-tuple-element.14), calls=%async_computation.2 | async-start | bytes 262144 | tf_op jit(solution)/shard_map/all_to_all | solution.py:31

commit v5 on v3

v5 whole, which is shorter than its diff:
```python
import functools

import jax
import jax.numpy as jnp
from jax import lax
from jax.experimental import pallas as pl
from jax.experimental.pallas import tpu as pltpu
from jax.sharding import Mesh
from jax.sharding import PartitionSpec as P

FS = ("zh", "zl", "yh", "yl")
NEAR = ("zl", "yl", "x")
FAR = ("zh", "yh")
CLOSE = ("zl", "yl")
LAST = ("zl", "yl", "x", "c")

BETA_ONE = 0.9
BETA_TWO = 0.95
STEP_RATE = 0.01
EPSILON = 1e-08
NORM_FLOOR = 1e-06
BF = jnp.bfloat16
F32 = jnp.float32
FIRST = (((0,), (0,)), ((), ()))
LANES = 128
PART = 32
VMEM = pl.BlockSpec(memory_space=pltpu.VMEM)
ANY = pl.BlockSpec(memory_space=pltpu.HBM)
SMEM = pl.BlockSpec(memory_space=pltpu.SMEM)


def swap(pieces, axes):
    return lax.all_to_all(pieces, axes, 0, 0, tiled=True)


def shifted(value, axis, step):
    length = lax.axis_size(axis)
    return lax.ppermute(value, axis, [(i, (i + step) % length) for i in range(length)])


def split_two(v):
    high = v.astype(BF)
    return high, (v - high.astype(F32)).astype(BF)


def dot(a, b, dims=(((1,), (0,)), ((), ()))):
    return lax.dot_general(a, b, dims, preferred_element_type=F32)


def one_less_exp(v):
    series = 1.0 + v * 0.125
    for k in range(7, 1, -1):
        series = 1.0 + v * (1.0 / k) * series
    return jnp.where(v > -0.3, -v * series, 1.0 - jnp.exp(v))


def gate_signals(cot, totals):
    heads, tokens = cot.shape
    later = lax.broadcasted_iota(jnp.int32, (tokens, tokens), 0) >= lax.broadcasted_iota(
        jnp.int32, (tokens, tokens), 1
    )
    later = jnp.where(later, 1.0, 0.0).astype(BF)
    one = cot.astype(BF).astype(F32)
    rest = cot - one
    two = rest.astype(BF).astype(F32)
    parts = jnp.concatenate([one, two, rest - two, jnp.zeros_like(one)], axis=0).astype(BF)
    trailing = dot(parts, later)
    trailing = trailing[2 * heads : 3 * heads] + trailing[heads : 2 * heads] + trailing[:heads]
    lane = lax.broadcasted_iota(jnp.int32, totals.shape, 1)
    gate = totals - jnp.where(lane == 0, 0.0, pltpu.roll(totals, 1, 1))
    return (trailing * one_less_exp(gate)).astype(BF)


def lane_blocks(shape):
    return lax.broadcasted_iota(jnp.int32, shape, len(shape) - 1) // PART


def turn(value, blocks):
    blocks = blocks % (LANES // PART)
    return pltpu.roll(value, blocks * PART, 1) if blocks else value


def turn_by(value, blocks):
    count = LANES // PART
    return pltpu.roll(value, lax.rem(blocks + 2 * count, count) * PART, 1)


def first_kernel(
    sizes, x_ref, q_ref, cot_ref, tot_ref, out_ref, x_held, q_held, out_held, gate_held, x_sem, q_sem, out_sem
):
    nz, nzl, ny, nyl, nx, own = sizes
    wide = x_held.shape[2]
    heads = gate_held.shape[1]
    copies = []
    q_copy = pltpu.make_async_copy(q_ref, q_held, q_sem)
    q_copy.start()
    for z in range(nz):
        copy = pltpu.make_async_copy(x_ref.at[:, z * wide : (z + 1) * wide], x_held.at[z], x_sem.at[z])
        copy.start()
        copies.append(copy)
    signal = gate_signals(cot_ref[...], tot_ref[...])
    q_copy.wait()
    lane = lane_blocks((own, LANES))
    sends = []
    for z in range(nz):
        copies[z].wait()
        block = x_held[z]
        part = dot(block, q_held[...], FIRST)
        for yh in range(ny):
            to = slice(yh * own, (yh + 1) * own)
            for q in range(nx):
                turned = []
                for j in range(nzl * nyl):
                    row = ((j // nyl * ny + yh) * nyl + j % nyl) * own
                    turned.append(turn(part[row : row + own, q * LANES : (q + 1) * LANES], j))
                for t in range(nzl * nyl):
                    piece = turned[0]
                    for j in range(1, nzl * nyl):
                        piece = jnp.where(lane == (t + j) % (nzl * nyl), turned[j], piece)
                    out_held[z, t * nx + q, to, :] = piece.astype(BF)
        target = out_ref.at[:, z * ny * own : (z + 1) * ny * own, :]
        send = pltpu.make_async_copy(out_held.at[z], target, out_sem.at[z])
        send.start()
        sends.append(send)
        gates = dot(signal, block).astype(BF)
        for k in range(wide // LANES):
            gate_held[z * (wide // LANES) + k] = gates[:, k * LANES : (k + 1) * LANES]
    target = out_ref.at[:, nz * ny * own : nz * ny * own + heads, :]
    send = pltpu.make_async_copy(gate_held, target, out_sem.at[nz])
    send.start()
    sends.append(send)
    for send in sends:
        send.wait()


def second_kernel(own, in_ref, out_ref):
    far, rows = out_ref.shape[:2]
    for k in range(far + 1):
        cut = slice(k * own, (k + 1) * own) if k < far else slice(far * own, in_ref.shape[1])
        summed = in_ref[0, cut].astype(F32)
        for i in range(1, in_ref.shape[0]):
            summed = summed + in_ref[i, cut].astype(F32)
        if k < far:
            out_ref[k, :own, :] = summed.astype(BF)
        else:
            for j in range(far):
                out_ref[j, own:, :] = summed.astype(BF)


def four_factors(p_ref, t):
    return jnp.concatenate([p_ref[j ^ t] for j in range(p_ref.shape[0])], axis=0)


def two_halves(value, out_ref):
    top = lax.broadcasted_iota(jnp.int32, (8, LANES), 0) < 4
    for g in range(out_ref.shape[0] // 2):
        rows = value[8 * g : 8 * g + 8]
        high = rows.astype(BF).astype(F32)
        low = rows - high
        out_ref[2 * g] = jnp.where(top, high, pltpu.roll(low, 4, 0)).astype(BF)
        out_ref[2 * g + 1] = jnp.where(top, pltpu.roll(high, 4, 0), low).astype(BF)


def third_kernel(norming, at_ref, in_ref, p_ref, gradient_ref, out_ref, gate_ref):
    own = p_ref.shape[1]
    count = p_ref.shape[0]
    summed = in_ref[0].astype(F32)
    for k in range(1, in_ref.shape[0]):
        summed = summed + in_ref[k].astype(F32)
    summed = summed * norming
    gate_ref[...] = summed[own:]
    gradient = turn_by(summed[:own], -at_ref[2])
    gradient_ref[...] = gradient
    factor = four_factors(p_ref, at_ref[2])
    high, low = split_two(jnp.concatenate([turn(gradient, -j) for j in range(count)], axis=0))
    rank = dot(factor, high, FIRST) + dot(factor, low, FIRST)
    block = rank.shape[0] // count
    lane = lane_blocks((block, LANES))
    packed = rank[:block]
    for u in range(1, count):
        packed = jnp.where(lane == u, turn(rank[u * block : (u + 1) * block], u), packed)
    two_halves(packed, out_ref)


def rank_kernel(in_ref, out_ref):
    summed = in_ref[0].astype(F32)
    for k in range(1, in_ref.shape[0]):
        summed = summed + in_ref[k].astype(F32)
    summed = summed + pltpu.roll(summed, 4, 0)
    high = summed.astype(BF).astype(F32)
    top = lax.broadcasted_iota(jnp.int32, (8, LANES), 0) < 4
    piece = jnp.where(top, high, summed - high).astype(BF)
    for k in range(out_ref.shape[0]):
        out_ref[k] = piece


def fourth_kernel(sizes, at_ref, in_ref, moments_ref, p_ref, gradient_ref, gates_ref, out_ref):
    nx, nc = sizes
    count, own = p_ref.shape[:2]
    top = lax.broadcasted_iota(jnp.int32, (8, LANES), 0) < 4
    rows = []
    for g in range(in_ref.shape[0] // 2):
        even, odd = in_ref[2 * g].astype(F32), in_ref[2 * g + 1].astype(F32)
        even = even + pltpu.roll(even, 4, 0)
        odd = odd + pltpu.roll(odd, 4, 0)
        rows.append(jnp.where(top, even, odd))
    projected = jnp.concatenate(rows, axis=0)
    block = projected.shape[0]
    lane = lane_blocks((2 * block, LANES))
    moments = moments_ref[0]
    for s in range(nx):
        u = lax.rem(at_ref[0] + nx - s, nx)
        moments = jnp.where(lane == u, turn_by(moments_ref[s], u - at_ref[2]), moments)
    mean = BETA_ONE * moments[:block] + (1.0 - BETA_ONE) * projected
    square = BETA_TWO * moments[block:] + (1.0 - BETA_TWO) * projected * projected
    direction = mean / (jnp.sqrt(square) + EPSILON)
    sums = [
        jnp.sum(direction * direction, axis=0, keepdims=True),
        jnp.sum(projected * projected, axis=0, keepdims=True),
    ]
    sums = jnp.concatenate(sums, axis=0)
    one = sums.astype(BF).astype(F32)
    two = (sums - one).astype(BF).astype(F32)
    sums = jnp.concatenate([one, two, sums - one - two, jnp.zeros((2, LANES), F32)], axis=0).astype(BF)
    lane = lane_blocks((block, LANES))
    both = [jnp.where(lane == 0, turn(direction, -u), turn(projected, 1 - u)) for u in range(count)]
    high, low = split_two(jnp.concatenate(both, axis=0))
    factor = four_factors(p_ref, at_ref[2])
    lifted = dot(factor, high) + dot(factor, low)
    lane = lane_blocks((own, LANES))
    gates = gates_ref[...].astype(BF)
    gradient = gradient_ref[...]
    for x in range(nx):
        tail = jnp.where(lane == 2, turn(projected[:own], 2 - x), turn(projected[own:], 3 - x))
        for j in range(count):
            piece = lifted[j * own : (j + 1) * own]
            piece = jnp.where(lane == 1, piece - turn(gradient, 1 - j), piece)
            piece = jnp.where(lane < 2, piece, tail).astype(BF)
            for c in range(nc):
                k = (j * nx + x) * nc + c
                out_ref[k, :own] = piece
                out_ref[k, own : own + 8] = gates
                out_ref[k, own + 8 :] = sums


def last_kernel(
    sizes,
    at_ref,
    in_ref,
    master_ref,
    mean_ref,
    square_ref,
    gate_mean_ref,
    gate_square_ref,
    update_ref,
    new_ref,
    copy_ref,
    mean_out,
    square_out,
    gate_update_ref,
    average_ref,
    energy_ref,
):
    count, nx, nc = sizes
    own = master_ref.shape[0]
    sums = in_ref[0, own + 8 :].astype(F32)
    for k in range(1, in_ref.shape[0]):
        sums = sums + in_ref[k, own + 8 :].astype(F32)
    sums = sums[0:2] + sums[2:4] + sums[4:6]
    direction_squares = jnp.sum(sums[0:1], axis=1, keepdims=True)
    projected_squares = jnp.sum(sums[1:2], axis=1, keepdims=True)
    balance = jnp.sqrt(direction_squares / (projected_squares + NORM_FLOOR))
    lane = lane_blocks((own, LANES))
    for x in range(nx):
        update, upper, lower = None, None, None
        for t in range(count):
            k = (t * nx + x) * nc + at_ref[1]
            piece = in_ref[k, :own].astype(F32)
            term = turn(piece - balance * turn(piece, -1), t)
            above, below = turn(piece, t - 2), turn(piece, t - 3)
            update = term if t == 0 else jnp.where(lane == t, term, update)
            upper = above if t == 0 else jnp.where(lane == t, above, upper)
            lower = below if t == 0 else jnp.where(lane == t, below, lower)
            g = in_ref[k, own : own + 8].astype(F32)
            place = slice((t * nx + x) * LANES, (t * nx + x + 1) * LANES)
            average = BETA_ONE * gate_mean_ref[:, place] + (1.0 - BETA_ONE) * g
            energy = BETA_TWO * gate_square_ref[:, place] + (1.0 - BETA_TWO) * g * g
            average_ref[:, place] = average
            energy_ref[:, place] = energy
            gate_update_ref[:, place] = average / (jnp.sqrt(energy) + EPSILON)
        cut = slice(x * LANES, (x + 1) * LANES)
        update_ref[:, cut] = update
        new = master_ref[:, cut] - STEP_RATE * update
        new_ref[:, cut] = new
        copy_ref[:, cut] = new.astype(BF)
        p = jnp.concatenate([upper, lower], axis=0)
        mean_out[:, cut] = BETA_ONE * mean_ref[:, cut] + (1.0 - BETA_ONE) * p
        square_out[:, cut] = BETA_TWO * square_ref[:, cut] + (1.0 - BETA_TWO) * p * p


def near_memory(value):
    return pltpu.with_memory_space_constraint(value, pltpu.VMEM)


def per_device(
    attention_input,
    query_cotangent,
    gate_cotangent,
    gate_totals,
    projector,
    query_master,
    lowrank_mean,
    lowrank_square,
    gating_mean,
    gating_square,
):
    nz, ny, nzl, nyl, nx, nc = (lax.axis_size(a) for a in ("zh", "yh", "zl", "yl", "x", "c"))
    far, near = nz * ny, nzl * nyl * nx
    count = nzl * nyl
    tokens, width = attention_input.shape
    columns = query_cotangent.shape[1]
    heads = gate_cotangent.shape[0]
    own, rank = projector.shape
    block = rank // nx
    norming = 1.0 / (tokens * far * near) ** 0.5
    shape = jax.ShapeDtypeStruct
    at = jnp.stack([lax.axis_index(a) for a in ("x", "c", CLOSE)]).astype(jnp.int32)

    wide = nzl * ny * nyl * own
    first = pl.pallas_call(
        functools.partial(first_kernel, (nz, nzl, ny, nyl, nx, own)),
        out_shape=shape((near, far * own + heads, LANES), BF),
        in_specs=[ANY, ANY, VMEM, VMEM],
        out_specs=ANY,
        scratch_shapes=[
            pltpu.VMEM((nz, tokens, wide), BF),
            pltpu.VMEM((tokens, columns), BF),
            pltpu.VMEM((nz, near, ny * own, LANES), BF),
            pltpu.VMEM((near, heads, LANES), BF),
            pltpu.SemaphoreType.DMA((nz,)),
            pltpu.SemaphoreType.DMA,
            pltpu.SemaphoreType.DMA((nz + 1,)),
        ],
        name="first",
    )(attention_input, query_cotangent, gate_cotangent, gate_totals)
    first = swap(first, NEAR)
    mine = jnp.concatenate(
        [lowrank_mean.reshape(block, nx, LANES), lowrank_square.reshape(block, nx, LANES)]
    ).transpose(1, 0, 2)
    place = lax.axis_index("x")
    pieces = [lax.dynamic_index_in_dim(mine, lax.rem(place + s, nx), 0, False) for s in range(nx)]
    moments = jnp.stack([pieces[0], *(shifted(pieces[s], "x", s) for s in range(1, nx))])
    neighbours = [lax.ppermute(projector, CLOSE, [(i, i ^ e) for i in range(count)]) for e in range(1, count)]
    factors = jnp.stack([projector, *neighbours])
    first, moments, factors = lax.optimization_barrier((first, moments, factors))

    second = pl.pallas_call(
        functools.partial(second_kernel, own),
        out_shape=pltpu.VMEM((far, own + heads, LANES), BF),
        in_specs=[VMEM],
        out_specs=VMEM,
        name="second",
    )(near_memory(first))
    second = swap(second, FAR)

    gradient, third, gates = pl.pallas_call(
        functools.partial(third_kernel, norming),
        out_shape=(
            pltpu.VMEM((own, LANES), F32),
            pltpu.VMEM((far, 8, LANES), BF),
            pltpu.VMEM((heads, LANES), F32),
        ),
        in_specs=[SMEM, VMEM, VMEM],
        out_specs=(VMEM, VMEM, VMEM),
        name="third",
    )(at, near_memory(second), near_memory(factors))
    third = swap(third, FAR)

    ranked = pl.pallas_call(
        rank_kernel,
        out_shape=pltpu.VMEM((far, 8, LANES), BF),
        in_specs=[VMEM],
        out_specs=VMEM,
        name="ranked",
    )(near_memory(third))
    ranked = swap(ranked, FAR)

    fourth = pl.pallas_call(
        functools.partial(fourth_kernel, (nx, nc)),
        out_shape=pltpu.VMEM((count * nx * nc, own + 16, LANES), BF),
        in_specs=[SMEM, VMEM, VMEM, VMEM, VMEM, VMEM],
        out_specs=VMEM,
        name="fourth",
    )(
        at,
        near_memory(ranked),
        near_memory(moments),
        near_memory(factors),
        near_memory(gradient),
        near_memory(gates),
    )
    fourth = swap(fourth, LAST)

    return pl.pallas_call(
        functools.partial(last_kernel, (count, nx, nc)),
        out_shape=(
            shape((own, columns), F32),
            shape((own, columns), F32),
            shape((own, columns), BF),
            shape((block, columns), F32),
            shape((block, columns), F32),
            shape((heads, width), F32),
            shape((heads, width), F32),
            shape((heads, width), F32),
        ),
        in_specs=[SMEM, *[VMEM] * 6],
        out_specs=(VMEM,) * 8,
        name="last",
    )(at, near_memory(fourth), query_master, lowrank_mean, lowrank_square, gating_mean, gating_square)


def solution(mesh):
    split = Mesh(
        mesh.devices.reshape(4, 2, 4, 2, mesh.shape["rep"], mesh.shape["tp"]),
        ("zh", "zl", "yh", "yl", "x", "c"),
    )
    in_specs = (
        P((*FS, "x"), None),
        P((*FS, "x"), "c"),
        P("c", (*FS, "x")),
        P("c", (*FS, "x")),
        P(FS, None),
        P(FS, "c"),
        P("x", "c"),
        P("x", "c"),
        P("c", None),
        P("c", None),
    )
    out_specs = (
        P(FS, "c"),
        P(FS, "c"),
        P(FS, "c"),
        P("x", "c"),
        P("x", "c"),
        P("c", None),
        P("c", None),
        P("c", None),
    )
    return jax.shard_map(
        per_device, mesh=split, in_specs=in_specs, out_specs=out_specs, check_vma=False
    )
```

time: 138 us -> 127 us (0.920)
  blocking collectives: 20.8 us -> 48.6 us
  waiting for transfers between devices: 48.2 us -> 23.3 us
  starting transfers between devices: 53.3 us -> 40.7 us
  Pallas kernels: 13.4 us -> 11.8 us
    all_to_all x4 -> x2, waiting for transfers between devices: 41.6 us -> 10.9 us  [swap(): return lax.all_to_all(pieces, axes, 0, 0, tiled=True)]
    all_to_all x1 -> x3, blocking collectives: 20.8 us -> 48.6 us  [swap(): return lax.all_to_all(pieces, axes, 0, 0, tiled=True)]
    all_to_all x4 -> x2, starting transfers between devices: 39.2 us -> 22.3 us  [swap(): return lax.all_to_all(pieces, axes, 0, 0, tiled=True)]
    ppermute x0 -> x3, starting transfers between devices: none -> 8.37 us  [per_device(): lax.ppermute(projector, CLOSE, [(i, i ^ e) for i in range(count)])]
    ppermute x0 -> x3, waiting for transfers between devices: none -> 8.28 us  [per_device(): lax.ppermute(projector, CLOSE, [(i, i ^ e) for i in range(count)])]
    ppermute x5 -> x3, starting transfers between devices: 14.1 us -> 10 us  [shifted(): lax.ppermute(value, axis, [(i, (i + step) % length) for i in range(length)])]
    ppermute x5 -> x3, waiting for transfers between devices: 6.64 us -> 4.14 us  [shifted(): lax.ppermute(value, axis, [(i, (i + step) % length) for i in range(length)])]
  transfers between devices with their start and end apart: 9 -> 8, of which waited for: 7 -> 3; matrix products, arithmetic and copies ran while one was open for 0% -> 1% of each run, Pallas kernels for 0% -> 0%
where the time goes in v5:
time: 127 us; the launch traced here: 126 us
  blocking collectives  48.6 us (38%)
  starting transfers between devices  40.7 us (32%)
  waiting for transfers between devices  23.3 us (18%)
  Pallas kernels  11.8 us (9%)
    all_to_all x3, blocking collectives, swap(): return lax.all_to_all(pieces, axes, 0, 0, tiled=True)  48.6 us
    all_to_all x2, starting transfers between devices, swap(): return lax.all_to_all(pieces, axes, 0, 0, tiled=True)  22.3 us
    all_to_all x2, waiting for transfers between devices, swap(): return lax.all_to_all(pieces, axes, 0, 0, tiled=True)  10.9 us
    ppermute x3, starting transfers between devices, shifted(): lax.ppermute(value, axis, [(i, (i + step) % length) for i in range(length)])  10 us
    ppermute x3, starting transfers between devices, per_device(): lax.ppermute(projector, CLOSE, [(i, i ^ e) for i in range(count)])  8.37 us
    ppermute x3, waiting for transfers between devices, per_device(): lax.ppermute(projector, CLOSE, [(i, i ^ e) for i in range(count)])  8.28 us
    pallas_call x1, Pallas kernels, per_device(): pl.pallas_call(functools.partial(first_kernel, (nz, nzl, ny, nyl, nx, own...  6.52 us
    ppermute x3, waiting for transfers between devices, shifted(): lax.ppermute(value, axis, [(i, (i + step) % length) for i in range(length)])  4.14 us
  transfers between devices with their start and end apart: 8, of which 3 were waited for; matrix products, arithmetic and copies ran while one was open for 1% of the time, Pallas kernels for 0%

profile of v5, /device:TPU:1, one launch (start us, length us, event | category | flops | bytes accessed | tf_op | source)
XLA Modules:
  0.0 125.9 jit_solution(17499512511528582583)
XLA Ops:
  0.6 6.5 %first.1 = bf16[16,520,128]{2,1,0:T(8,128)(2,1)} custom-call(bf16[768,2048]{1,0:T(8,128)(2,1)} %x_ref.1, bf16[768,512]{1,0:T(8,128)(2,1)} %q_ref.1, f32[8,768]{1,0:T(8,128)} %cot_ref.1, f32[8,768]{1,0:T(8,128)} %tot_ref.1), custom_call_target="tpu_custom_call" | custom-call | tf_op jit(solution)/shard_map/first/pallas_call | solution.py:330
  7.2 0.0 copy-start.2
  7.2 0.0 copy-start
  7.2 0.0 copy-start.1
  7.2 7.9 %all-to-all-start = ((bf16[16,520,128]{2,1,0:T(8,128)(2,1)}), bf16[16,520,128]{2,1,0:T(8,128)(2,1)S(1)}, u32[]{:S(2)}, u32[]{:S(2)}) async-start(bf16[16,520,128]{2,1,0:T(8,128)(2,1)} %first.1), calls=%async_computation | async-start | bytes 4259840 | tf_op jit(solution)/shard_map/all_to_all | solution.py:33
  15.1 0.0 copy-done.2
  15.1 4.2 %collective-permute-start.5 = (bf16[32,256]{1,0:T(8,128)(2,1)S(1)}, bf16[32,256]{1,0:T(8,128)(2,1)S(1)}, u32[]{:S(2)}, u32[]{:S(2)}) collective-permute-start(bf16[32,256]{1,0:T(8,128)(2,1)S(1)} %copy-done.2), channel_id=1, source_target_pairs={{0,72},{8,64},{64,8},{72,0},{1,73},{9,65},{65,9},{73,1},{2,74},{10... | collective-permute-start | bytes 49160 | tf_op jit(solution)/shard_map/ppermute | solution.py:353
  19.3 2.2 %collective-permute-start.4 = (bf16[32,256]{1,0:T(8,128)(2,1)S(1)}, bf16[32,256]{1,0:T(8,128)(2,1)S(1)}, u32[]{:S(2)}, u32[]{:S(2)}) collective-permute-start(bf16[32,256]{1,0:T(8,128)(2,1)S(1)} %copy-done.2), channel_id=1, source_target_pairs={{0,64},{8,72},{64,0},{72,8},{1,65},{9,73},{65,1},{73,9},{2,66},{10... | collective-permute-start | bytes 49160 | tf_op jit(solution)/shard_map/ppermute | solution.py:353
  21.5 2.0 %collective-permute-start.3 = (bf16[32,256]{1,0:T(8,128)(2,1)S(1)}, bf16[32,256]{1,0:T(8,128)(2,1)S(1)}, u32[]{:S(2)}, u32[]{:S(2)}) collective-permute-start(bf16[32,256]{1,0:T(8,128)(2,1)S(1)} %copy-done.2), channel_id=1, source_target_pairs={{0,8},{8,0},{64,72},{72,64},{1,9},{9,1},{65,73},{73,65},{2,10},{10... | collective-permute-start | bytes 49160 | tf_op jit(solution)/shard_map/ppermute | solution.py:353
  23.6 0.0 copy-done
  23.6 0.0 copy-done.1
  23.6 4.5 %collective-permute-start.2 = (f32[128,128]{1,0:T(8,128)S(1)}, f32[128,128]{1,0:T(8,128)S(1)}, u32[]{:S(2)}, u32[]{:S(2)}) collective-permute-start(f32[128,128]{1,0:T(8,128)S(1)} %get-tuple-element.21), channel_id=1, source_target_pairs={{0,6},{2,0},{4,2},{6,4},{1,7},{3,1},{5,3},{7,5},{8,14},{10,8},{12,... | collective-permute-start | bytes 196616 | tf_op jit(solution)/shard_map/ppermute | solution.py:38
  28.1 2.5 %collective-permute-start.1 = (f32[128,128]{1,0:T(8,128)S(1)}, f32[128,128]{1,0:T(8,128)S(1)}, u32[]{:S(2)}, u32[]{:S(2)}) collective-permute-start(f32[128,128]{1,0:T(8,128)S(1)} %get-tuple-element.22), channel_id=1, source_target_pairs={{0,4},{2,6},{4,0},{6,2},{1,5},{3,7},{5,1},{7,3},{8,12},{10,14},{12... | collective-permute-start | bytes 196616 | tf_op jit(solution)/shard_map/ppermute | solution.py:38
  30.6 8.3 %collective-permute-done.5 = bf16[32,256]{1,0:T(8,128)(2,1)S(1)} collective-permute-done((bf16[32,256]{1,0:T(8,128)(2,1)S(1)}, bf16[32,256]{1,0:T(8,128)(2,1)S(1)}, u32[]{:S(2)}, u32[]{:S(2)}) %collective-permute-start.5) | collective-permute-done | bytes 16416 | tf_op jit(solution)/shard_map/ppermute | solution.py:353
  38.9 3.1 %collective-permute-start = (f32[128,128]{1,0:T(8,128)S(1)}, f32[128,128]{1,0:T(8,128)S(1)}, u32[]{:S(2)}, u32[]{:S(2)}) collective-permute-start(f32[128,128]{1,0:T(8,128)S(1)} %get-tuple-element.23), channel_id=1, source_target_pairs={{0,2},{2,4},{4,6},{6,0},{1,3},{3,5},{5,7},{7,1},{8,10},{10,12},{12... | collective-permute-start | bytes 196616 | tf_op jit(solution)/shard_map/ppermute | solution.py:38
  42.0 0.0 collective-permute-done.4
  42.0 0.0 collective-permute-done.3
  42.0 0.0 collective-permute-done.2
  42.0 0.0 collective-permute-done.1
  42.0 4.1 %collective-permute-done = f32[128,128]{1,0:T(8,128)S(1)} collective-permute-done((f32[128,128]{1,0:T(8,128)S(1)}, f32[128,128]{1,0:T(8,128)S(1)}, u32[]{:S(2)}, u32[]{:S(2)}) %collective-permute-start) | collective-permute-done | bytes 65568 | tf_op jit(solution)/shard_map/ppermute | solution.py:38
  46.2 0.0 all-to-all-done.in_ref
  46.2 0.9 second.1
  47.2 14.4 %all-to-all-start.1 = ((bf16[16,40,128]{2,1,0:T(8,128)(2,1)}), bf16[16,40,128]{2,1,0:T(8,128)(2,1)S(1)}, u32[]{:S(2)}, u32[]{:S(2)}) async-start(bf16[16,40,128]{2,1,0:T(8,128)(2,1)} %second.1), calls=%async_computation.1 | async-start | bytes 327680 | tf_op jit(solution)/shard_map/all_to_all | solution.py:33
  61.6 0.6 pad_add_fusion.at_ref
  62.2 10.9 %all-to-all-done.1.in_ref = bf16[16,40,128]{2,1,0:T(8,128)(2,1)S(1)} async-done(((bf16[16,40,128]{2,1,0:T(8,128)(2,1)}), bf16[16,40,128]{2,1,0:T(8,128)(2,1)S(1)}, u32[]{:S(2)}, u32[]{:S(2)}) %all-to-all-start.1) | async-done | bytes 163872 | tf_op jit(solution)/shard_map/all_to_all | solution.py:33
  73.0 1.1 third.1
  74.1 14.1 %all_to_all.25.in_ref = bf16[16,8,128]{2,1,0:T(8,128)(2,1)S(1)} all-to-all(bf16[16,8,128]{2,1,0:T(8,128)(2,1)S(1)} %get-tuple-element.16), channel_id=1, replica_groups=mesh['zh'=4,'zl'=2,'yh'=4,'yl'=2,'x'=4,'c'=2] {'zh','yh'}, dimensions={0} | all-to-all | bytes 65536 | tf_op jit(solution)/shard_map/all_to_all | solution.py:33
  88.3 13.8 %all_to_all.26.in_ref = bf16[16,8,128]{2,1,0:T(8,128)(2,1)S(1)} all-to-all(bf16[16,8,128]{2,1,0:T(8,128)(2,1)S(1)} %ranked.1), channel_id=1, replica_groups=mesh['zh'=4,'zl'=2,'yh'=4,'yl'=2,'x'=4,'c'=2] {'zh','yh'}, dimensions={0} | all-to-all | bytes 65536 | tf_op jit(solution)/shard_map/all_to_all | solution.py:33
  102.1 1.1 fourth.1
  103.2 20.6 %all_to_all.27.in_ref = bf16[32,48,128]{2,1,0:T(8,128)(2,1)S(1)} all-to-all(bf16[32,48,128]{2,1,0:T(8,128)(2,1)S(1)} %fourth.1), channel_id=1, replica_groups=mesh['zh'=4,'zl'=2,'yh'=4,'yl'=2,'x'=4,'c'=2] {'zl','yl','x','c'}, dimensions={0} | all-to-all | bytes 786432 | tf_op jit(solution)/shard_map/all_to_all | solution.py:33
  123.8 2.1 %last.1 = (f32[32,512]{1,0:T(8,128)}, f32[32,512]{1,0:T(8,128)}, bf16[32,512]{1,0:T(8,128)(2,1)}, f32[64,512]{1,0:T(8,128)}, f32[64,512]{1,0:T(8,128)}, /*index=...) custom-call(s32[3]{0:T(128)} %pad_add_fusion.at_ref, bf16[32,48,128]{2,1,0:T(8,128)(2,1)S(1)} %all_to_all.27.in_ref, ...), custom_call_target="tpu_custom_call" | custom-call | tf_op jit(solution)/shard_map/last/pallas_call | solution.py:404
  (6 shorter events, 0.1 us)
Async XLA Ops:
  7.2 8.0 %copy-start.2 = (bf16[32,256]{1,0:T(8,128)(2,1)S(1)}, bf16[32,256]{1,0:T(8,128)(2,1)}, u32[]{:S(2)}) copy-start(bf16[32,256]{1,0:T(8,128)(2,1)} %param.14) | copy-start | bytes 49156
  7.2 16.4 %copy-start = (f32[64,512]{1,0:T(8,128)S(1)}, f32[64,512]{1,0:T(8,128)}, u32[]{:S(2)}) copy-start(f32[64,512]{1,0:T(8,128)} %mean_ref.1) | copy-start | bytes 393220
  7.2 16.4 %copy-start.1 = (f32[64,512]{1,0:T(8,128)S(1)}, f32[64,512]{1,0:T(8,128)}, u32[]{:S(2)}) copy-start(f32[64,512]{1,0:T(8,128)} %square_ref.1) | copy-start | bytes 393220
  7.2 39.0 %all-to-all-start = ((bf16[16,520,128]{2,1,0:T(8,128)(2,1)}), bf16[16,520,128]{2,1,0:T(8,128)(2,1)S(1)}, u32[]{:S(2)}, u32[]{:S(2)}) async-start(bf16[16,520,128]{2,1,0:T(8,128)(2,1)} %first.1), calls=%async_computation | async-start | bytes 4259840 | tf_op jit(solution)/shard_map/all_to_all | solution.py:33
  15.1 23.8 %collective-permute-start.5 = (bf16[32,256]{1,0:T(8,128)(2,1)S(1)}, bf16[32,256]{1,0:T(8,128)(2,1)S(1)}, u32[]{:S(2)}, u32[]{:S(2)}) collective-permute-start(bf16[32,256]{1,0:T(8,128)(2,1)S(1)} %copy-done.2), channel_id=1, source_target_pairs={{0,72},{8,64},{64,8},{72,0},{1,73},{9,65},{65,9},{73,1},{2,74},{10... | collective-permute-start | bytes 49160 | tf_op jit(solution)/shard_map/ppermute | solution.py:353
  19.3 22.7 %collective-permute-start.4 = (bf16[32,256]{1,0:T(8,128)(2,1)S(1)}, bf16[32,256]{1,0:T(8,128)(2,1)S(1)}, u32[]{:S(2)}, u32[]{:S(2)}) collective-permute-start(bf16[32,256]{1,0:T(8,128)(2,1)S(1)} %copy-done.2), channel_id=1, source_target_pairs={{0,64},{8,72},{64,0},{72,8},{1,65},{9,73},{65,1},{73,9},{2,66},{10... | collective-permute-start | bytes 49160 | tf_op jit(solution)/shard_map/ppermute | solution.py:353
  21.5 20.5 %collective-permute-start.3 = (bf16[32,256]{1,0:T(8,128)(2,1)S(1)}, bf16[32,256]{1,0:T(8,128)(2,1)S(1)}, u32[]{:S(2)}, u32[]{:S(2)}) collective-permute-start(bf16[32,256]{1,0:T(8,128)(2,1)S(1)} %copy-done.2), channel_id=1, source_target_pairs={{0,8},{8,0},{64,72},{72,64},{1,9},{9,1},{65,73},{73,65},{2,10},{10... | collective-permute-start | bytes 49160 | tf_op jit(solution)/shard_map/ppermute | solution.py:353
  23.6 18.4 %collective-permute-start.2 = (f32[128,128]{1,0:T(8,128)S(1)}, f32[128,128]{1,0:T(8,128)S(1)}, u32[]{:S(2)}, u32[]{:S(2)}) collective-permute-start(f32[128,128]{1,0:T(8,128)S(1)} %get-tuple-element.21), channel_id=1, source_target_pairs={{0,6},{2,0},{4,2},{6,4},{1,7},{3,1},{5,3},{7,5},{8,14},{10,8},{12,... | collective-permute-start | bytes 196616 | tf_op jit(solution)/shard_map/ppermute | solution.py:38
  28.1 13.9 %collective-permute-start.1 = (f32[128,128]{1,0:T(8,128)S(1)}, f32[128,128]{1,0:T(8,128)S(1)}, u32[]{:S(2)}, u32[]{:S(2)}) collective-permute-start(f32[128,128]{1,0:T(8,128)S(1)} %get-tuple-element.22), channel_id=1, source_target_pairs={{0,4},{2,6},{4,0},{6,2},{1,5},{3,7},{5,1},{7,3},{8,12},{10,14},{12... | collective-permute-start | bytes 196616 | tf_op jit(solution)/shard_map/ppermute | solution.py:38
  38.9 7.3 %collective-permute-start = (f32[128,128]{1,0:T(8,128)S(1)}, f32[128,128]{1,0:T(8,128)S(1)}, u32[]{:S(2)}, u32[]{:S(2)}) collective-permute-start(f32[128,128]{1,0:T(8,128)S(1)} %get-tuple-element.23), channel_id=1, source_target_pairs={{0,2},{2,4},{4,6},{6,0},{1,3},{3,5},{5,7},{7,1},{8,10},{10,12},{12... | collective-permute-start | bytes 196616 | tf_op jit(solution)/shard_map/ppermute | solution.py:38
  47.2 25.9 %all-to-all-start.1 = ((bf16[16,40,128]{2,1,0:T(8,128)(2,1)}), bf16[16,40,128]{2,1,0:T(8,128)(2,1)S(1)}, u32[]{:S(2)}, u32[]{:S(2)}) async-start(bf16[16,40,128]{2,1,0:T(8,128)(2,1)} %second.1), calls=%async_computation.1 | async-start | bytes 327680 | tf_op jit(solution)/shard_map/all_to_all | solution.py:33
